TPU v7x, 768 devices: a whole 4x8x12 slice. The times are simulated.
768 devices in a mesh: sp: 192 (over z, y, core), tp: 4 (over x).
Axes of the slice: x: 4, y: 8, z: 12, core: 2. Of those that a mesh axis runs over, the one named last changes fastest.
Arguments:
- tokens: bfloat16 [1, 98304, 2048], P(None, ('sp', 'tp')), may hold values from -6 to 6
- input_norm_gain: float32 [2048], replicated, may hold values from 0.1 to 1.9
- query_weight: bfloat16 [2048, 1024], P(None, 'tp'), may hold values from -0.125 to 0.125
- forget_weight: bfloat16 [2048, 1024], P(None, 'tp'), may hold values from -0.125 to 0.125
- input_weight: bfloat16 [2048, 1024], P(None, 'tp'), may hold values from -0.125 to 0.125
- gate_weight: bfloat16 [2048, 1024], P(None, 'tp'), may hold values from -0.125 to 0.125
- slack: float32 [1024], P('tp'), may hold values from 0 to 0.06
- sudden_decay: float32 [1, 98304, 8], P(None, 'sp', 'tp'), may hold values from -0.75 to 0
- head_norm_gain: float32 [128], replicated, may hold values from 0.1 to 1.9
- output_weight: bfloat16 [1024, 2048], P(None, 'tp'), may hold values from -1.25 to 1.25
- output_norm_gain: float32 [2048], P('tp'), may hold values from 0.1 to 1.9
Outputs:
- mixer_output: bfloat16 [1, 98304, 2048], P(None, 'sp', 'tp')
All inputs are finite; a program needn't handle non-finite values.
Results may differ from a plain program's by a relative error of at most 0.0094.
Values may be sent and summed in bfloat16 or wider, within the bound.
A program may use at most 64 MiB of HBM per device.

v0:
```python
import jax
import jax.numpy as jnp
from jax import lax
from jax.sharding import Mesh
from jax.sharding import PartitionSpec as P

D = 2048
KEY = 128
BLOCK = 64
SP = ("sp_0", "sp_1", "sp_2")
SP_TP = ("sp_0", "sp_1", "sp_2", "tp")


epsilon = 1e-06
precise = lax.Precision.HIGHEST


def neutral_like(x, identity):
    return jax.tree.map(
        lambda a, e: jnp.broadcast_to(jnp.asarray(e, a.dtype), a.shape), x, identity
    )


def entering(x, axes, combine, identity):
    before = start = neutral_like(x, identity)
    so_far = x
    for axis in reversed(axes):
        devices, place = (lax.axis_size(axis), lax.axis_index(axis))
        pieces = jax.tree.map(lambda part: lax.all_gather(part, axis), so_far)
        inside, so_far = (start, start)
        for k in range(devices):
            passed = k < place
            so_far = combine(so_far, jax.tree.map(lambda part: part[k], pieces))
            inside = jax.tree.map(lambda new, old: jnp.where(passed, new, old), so_far, inside)
        before = combine(inside, before)
    return before


def laid_out(parts, dim):
    dims = list(parts.shape[1:])
    dims[dim] *= parts.shape[0]
    return jnp.moveaxis(parts, 0, dim).reshape(dims)


def copy_for_each(x, axis):
    copies = jnp.broadcast_to(x, (lax.axis_size(axis), *x.shape))
    return lax.all_to_all(copies, axis, split_axis=0, concat_axis=0, tiled=True)


def gathered_copies(x, axis, dim):
    return laid_out(copy_for_each(x, axis), dim)


def taken_together(x, axis):
    return copy_for_each(x, axis).sum(axis=0)


def normalize(tensor_in, gain_vec):
    tensor_in = tensor_in.astype(jnp.float32)
    return (
        tensor_in
        * lax.rsqrt(jnp.mean(tensor_in * tensor_in, axis=-1, keepdims=True) + epsilon)
        * gain_vec
    )


def setup_params(query_logits, forget_logits, input_logits, slack, sudden_decay):
    sequence_total, sequence_span, local_heads = sudden_decay.shape

    def heads_first(tensor):
        return (
            tensor.astype(jnp.float32)
            .reshape(sequence_total, sequence_span, local_heads, -1)
            .transpose(0, 2, 1, 3)
        )

    query_rows = heads_first(query_logits) * KEY ** (-0.5)
    incoming_weights = slack.reshape(local_heads, -1)[None, :, None, :] * jax.nn.sigmoid(
        -heads_first(forget_logits)
    )
    forget_logarithm = jnp.log1p(-incoming_weights) + sudden_decay.transpose(0, 2, 1)[:, :, :, None]
    return (query_rows, incoming_weights, heads_first(input_logits), forget_logarithm)


def block_pass(query_rows, incoming_weights, value_rows, forget_logarithm, initial):
    sequence_total, local_heads, sequence_span, key_width = query_rows.shape
    blocks_here = sequence_span // BLOCK

    def by_block(tensor):
        return tensor.reshape(
            sequence_total, local_heads, blocks_here, BLOCK, tensor.shape[3]
        ).transpose(2, 0, 1, 3, 4)

    causal = jnp.tril(jnp.ones((BLOCK, BLOCK), dtype=bool))

    def advance(carried, portions):
        query_blk, weight_blk, value_blk, forget_blk = portions
        running = jnp.cumsum(forget_blk, axis=2)
        lifted_q = query_blk * jnp.exp(running)
        lifted_k = weight_blk * jnp.exp(-running)
        scores = jnp.einsum("shtk,shuk->shtu", lifted_q, lifted_k, precision=precise)
        scores = jnp.where(causal, scores, 0.0)
        produced = jnp.einsum("shtu,shuv->shtv", scores, value_blk, precision=precise) + jnp.einsum(
            "shtk,shkv->shtv", lifted_q, carried, precision=precise
        )
        ending = running[:, :, -1:, :]
        carried = jnp.exp(ending[:, :, 0, :])[..., None] * carried + jnp.einsum(
            "shuk,shuv->shkv", weight_blk * jnp.exp(ending - running), value_blk, precision=precise
        )
        return (carried, produced)

    final_state, produced = lax.scan(
        advance,
        initial,
        (
            by_block(query_rows),
            by_block(incoming_weights),
            by_block(value_rows),
            by_block(forget_logarithm),
        ),
    )
    return (
        final_state,
        produced.transpose(1, 2, 0, 3, 4).reshape(
            sequence_total, local_heads, sequence_span, value_rows.shape[3]
        ),
    )


def gate_heads(produced, gate_raw, head_norm_gain):
    sequence_total, local_heads, sequence_span, val_width = produced.shape
    mean_sq = jnp.mean(produced * produced, axis=3, keepdims=True)
    scaled = produced * lax.rsqrt(mean_sq + epsilon) * head_norm_gain
    scaled = scaled.transpose(0, 2, 1, 3).reshape(
        sequence_total, sequence_span, local_heads * val_width
    )
    return (scaled * jax.nn.silu(gate_raw.astype(jnp.float32))).astype(jnp.bfloat16)


def join_states(earlier, later):
    earlier_decay, earlier_state = earlier
    later_decay, later_state = later
    return (
        earlier_decay + later_decay,
        jnp.exp(later_decay)[..., None] * earlier_state + later_state,
    )


def recurrence(query_rows, incoming_weights, value_rows, forget_logarithm):
    sequence_total, local_heads, sequence_span, key_width = query_rows.shape
    val_width = value_rows.shape[3]
    through = jnp.cumsum(forget_logarithm, axis=2)
    totals = through[:, :, -1, :]
    head_spans = (0, local_heads)
    head_from, head_upto = head_spans
    zero_state = jnp.zeros(
        (sequence_total, head_upto - head_from, key_width, val_width), jnp.float32
    )
    final_state, produced = block_pass(
        query_rows, incoming_weights, value_rows, forget_logarithm, zero_state
    )
    identity = (jnp.zeros_like(totals), jnp.zeros_like(final_state))
    incoming = entering((totals, final_state), SP, join_states, identity)
    incoming = incoming[1]
    readout = jnp.einsum(
        "shtk,shkv->shtv", query_rows * jnp.exp(through), incoming, precision=precise
    )
    outputs = produced + readout
    return outputs


def shards(
    tokens,
    input_norm_gain,
    query_weight,
    forget_weight,
    input_weight,
    gate_weight,
    slack,
    sudden_decay,
    head_norm_gain,
    output_weight,
    output_norm_gain,
):
    normed = normalize(tokens, input_norm_gain).astype(jnp.bfloat16)
    matrices = (query_weight, forget_weight, input_weight, gate_weight)
    portion = gathered_copies(normed, "tp", 1)
    joined = lax.optimization_barrier(
        jnp.concatenate(
            [
                jnp.einsum(
                    "std,dc->stc", portion, matrix, preferred_element_type=jnp.float32
                ).astype(jnp.bfloat16)
                for matrix in matrices
            ],
            axis=2,
        )
    )
    query_cols = query_weight.shape[1]
    input_cols = input_weight.shape[1]
    query_logits = joined[:, :, :query_cols]
    forget_logits = joined[:, :, query_cols : 2 * query_cols]
    input_logits = joined[:, :, 2 * query_cols : 2 * query_cols + input_cols]
    gate_raw = joined[:, :, 2 * query_cols + input_cols :]
    query_rows, incoming_weights, value_rows, forget_logarithm = setup_params(
        query_logits, forget_logits, input_logits, slack, sudden_decay
    )
    produced = recurrence(query_rows, incoming_weights, value_rows, forget_logarithm)
    gated_out = gate_heads(produced, gate_raw, head_norm_gain)
    projected = jnp.einsum(
        "stc,cd->std",
        gathered_copies(gated_out, "tp", 2),
        output_weight,
        preferred_element_type=jnp.float32,
    )
    squares = taken_together(jnp.sum(projected * projected, axis=2, keepdims=True), "tp")
    return (projected * lax.rsqrt(squares / D + epsilon) * output_norm_gain).astype(jnp.bfloat16)


def solution(mesh):
    torus = Mesh(mesh.devices.reshape(12, 8, 2, mesh.shape["tp"]), ("sp_0", "sp_1", "sp_2", "tp"))
    in_specs = (
        P(None, SP_TP, None),
        P(),
        P(None, "tp"),
        P(None, "tp"),
        P(None, "tp"),
        P(None, "tp"),
        P("tp"),
        P(None, SP, "tp"),
        P(),
        P(None, "tp"),
        P("tp"),
    )
    out_specs = P(None, SP, "tp")
    return jax.shard_map(
        shards, mesh=torus, in_specs=in_specs, out_specs=out_specs, check_vma=False
    )
```

profile of v0, /device:TPU:8, one launch (start us, length us, event | category | flops | bytes accessed | tf_op | source)
XLA Modules:
  0.0 225.5 jit_solution(5527419319717501406)
XLA Ops:
  6.5 1.3 fusion.30
  7.9 1.2 fusion.38
  9.1 1.6 broadcast_in_dim.26
  10.7 4.3 %all-to-all-start = ((bf16[4,1,128,2048]{3,2,1,0:T(8,128)(2,1)}), bf16[4,1,128,2048]{3,2,1,0:T(8,128)(2,1)S(1)}, u32[]{:S(2)}, u32[]{:S(2)}) async-start(bf16[4,1,128,2048]{3,2,1,0:T(8,128)(2,1)} %broadcast_in_dim.26), calls=%async_computation | async-start | bytes 4194304 | tf_op jit(solution)/shard_map/all_to_all | solution.py:47
  15.0 26.3 %all-to-all-done = bf16[4,1,128,2048]{3,2,1,0:T(8,128)(2,1)S(1)} async-done(((bf16[4,1,128,2048]{3,2,1,0:T(8,128)(2,1)}), bf16[4,1,128,2048]{3,2,1,0:T(8,128)(2,1)S(1)}, u32[]{:S(2)}, u32[]{:S(2)}) %all-to-all-start) | async-done | bytes 2097184 | tf_op jit(solution)/shard_map/all_to_all | solution.py:47
  41.3 2.1 fusion.29
  43.4 0.8 fusion.28
  44.2 0.4 copy-done.8
  44.6 0.8 fusion.27
  45.4 0.4 copy-done.9
  45.9 0.8 fusion.26
  46.8 1.1 convert_multiply_fusion.3
  48.3 0.3 fusion.42
  48.6 0.8 copy.49
  49.5 1.0 fusion.41
  50.6 1.2 copy.42
  51.8 22.1 %while.13 = (s32[]{:T(128)}, f32[1,2,128,128]{3,2,1,0:T(8,128)S(1)}, f32[8,1,2,64,128]{4,3,0,2,1:T(8,128)}, f32[8,1,2,64,128]{4,3,0,2,1:T(8,128)}, f32[8,1,2,64,...) while((s32[]{:T(128)}, ...), condition=%wide.region_3.4_spmd.clone, body=%wide.region_1.3_spmd.clone.sunk | while | flops 76787712 | bytes 1628290 | solution.py:112
  51.8 0.9 dynamic-slice_bitcast_fusion.2
  52.8 0.2 convolution_select_fusion.2
  53.3 0.9 fusion.222
  54.2 0.4 fusion.220
  54.6 0.9 dynamic-slice_bitcast_fusion.2
  55.6 0.2 convolution_select_fusion.2
  56.0 0.9 fusion.222
  56.9 0.4 fusion.220
  57.4 0.9 dynamic-slice_bitcast_fusion.2
  58.3 0.2 convolution_select_fusion.2
  58.8 0.9 fusion.222
  59.7 0.4 fusion.220
  60.1 0.9 dynamic-slice_bitcast_fusion.2
  61.1 0.2 convolution_select_fusion.2
  61.6 0.9 fusion.222
  62.5 0.4 fusion.220
  62.9 0.9 dynamic-slice_bitcast_fusion.2
  63.9 0.2 convolution_select_fusion.2
  64.3 0.9 fusion.222
  65.2 0.4 fusion.220
  65.7 0.9 dynamic-slice_bitcast_fusion.2
  66.6 0.2 convolution_select_fusion.2
  67.1 0.9 fusion.222
  68.0 0.4 fusion.220
  68.4 0.9 dynamic-slice_bitcast_fusion.2
  69.4 0.2 convolution_select_fusion.2
  69.8 0.9 fusion.222
  70.8 0.4 fusion.220
  71.2 0.9 dynamic-slice_bitcast_fusion.2
  72.1 0.2 convolution_select_fusion.2
  72.6 0.9 fusion.222
  73.5 0.4 fusion.220
  73.9 2.0 all-gather.1
  76.0 1.1 bitcast_add_fusion
  77.1 1.8 all-gather
  78.9 0.8 bitcast_add_fusion.12
  79.8 15.3 %all-gather.2 = f32[8,2,1,128]{3,1,2,0:T(2,128)S(1)} all-gather(f32[1,2,1,128]{3,1,2,0:T(2,128)S(1)} %get-tuple-element.107), channel_id=4, replica_groups=mesh['sp_0'=12,'sp_1'=8,'sp_2'=2,'tp'=4] {'sp_1'}, dimensions={0}, use_global_device_ids=true | all-gather | bytes 9216 | tf_op jit(solution)/shard_map/all_gather | solution.py:29
  95.1 32.8 %all-gather.6.cloned.1.call-done = f32[8,1,2,128,128]{4,3,2,1,0:T(8,128)} async-done(((f32[1,1,2,128,128]{4,3,2,1,0:T(8,128)}), f32[8,1,2,128,128]{4,3,2,1,0:T(8,128)}) %all-gather.6.cloned.1.call-update) | async-done | bytes 1048592 | tf_op jit(solution)/shard_map/all_gather | solution.py:29
  127.9 2.3 %multiply_add_fusion = f32[1,1,2,128,128]{4,3,2,1,0:T(8,128)} fusion(f32[8,1,2,128,128]{4,3,2,1,0:T(8,128)} %all-gather.6.cloned.1.call-done, f32[2,128]{1,0:T(2,128)S(1)} %get-tuple-element.131, f32[2,128]{1,0:T(2,128)S(1)} %get-tuple-element.130, f32[2,128]{1,0:T(2,128)S(1)} %get-tuple-element.129, f32[2,128]{1,0:T(2,128)S(1)} %get-tuple-element.128, ...), kind=kLoop, calls=%fused_computation.158 | loop fusion | flops 491520 | bytes 1187840 | tf_op jit(solution)/shard_map/add | solution.py:145
  130.3 1.2 copy.52
  131.6 24.2 %all_gather.27 = f32[12,1,2,128]{3,2,1,0:T(2,128)S(1)} all-gather(f32[1,1,2,128]{3,2,1,0:T(2,128)S(1)} %get-tuple-element.105), channel_id=1, replica_groups=mesh['sp_0'=12,'sp_1'=8,'sp_2'=2,'tp'=4] {'sp_0'}, dimensions={0}, use_global_device_ids=true | all-gather | bytes 13312 | tf_op jit(solution)/shard_map/all_gather | solution.py:29
  155.7 34.0 %all-gather.8.cloned.1.call-done = f32[12,1,2,128,128]{4,3,2,1,0:T(8,128)} async-done(((f32[1,1,2,128,128]{4,3,2,1,0:T(8,128)}), f32[12,1,2,128,128]{4,3,2,1,0:T(8,128)}) %all-gather.8.cloned.1.call-update) | async-done | bytes 1572880 | tf_op jit(solution)/shard_map/all_gather | solution.py:29
  189.7 3.4 %multiply_reduce_fusion.1 = (f32[2,512]{1,0:T(2,128)S(1)}, f32[2,512,128]{1,2,0:T(8,128)S(1)}) fusion(f32[2,512,128]{1,2,0:T(8,128)S(1)} %copy.52, f32[12,1,2,128,128]{4,3,2,1,0:T(8,128)} %all-gather.8.cloned.1.call-done, f32[8,1,2,128,128]{4,3,2,1,0:T(8,128)} %all-gather.6.cloned.1.call-done, f32[2,2,128,128]{3,2,1,0:T(8,128)S(1)} %all-gather.1, ...), kind=kOutput, calls=%fused_computation.69 | convolution fusion | flops 204045312 | bytes 5009430 | tf_op jit(solution)/shard_map/shtk,shkv->shtv/dot_general | solution.py:165
  193.6 15.5 %all_to_all.15 = bf16[4,1,512,256]{2,3,1,0:T(8,128)(2,1)S(1)} all-to-all(bf16[4,1,512,256]{2,3,1,0:T(8,128)(2,1)S(1)} %broadcast_in_dim.28), channel_id=1, replica_groups=mesh['sp_0'=12,'sp_1'=8,'sp_2'=2,'tp'=4] {'tp'}, dimensions={0} | all-to-all | bytes 2097152 | tf_op jit(solution)/shard_map/all_to_all | solution.py:47
  209.0 0.8 multiply_reduce_fusion
  209.8 7.7 %all_to_all.16 = f32[4,1,512,1]{2,3,1,0:T(1,128)S(1)} all-to-all(f32[4,1,512,1]{2,3,1,0:T(1,128)S(1)} %broadcast_in_dim.29), channel_id=1, replica_groups=mesh['sp_0'=12,'sp_1'=8,'sp_2'=2,'tp'=4] {'tp'}, dimensions={0} | all-to-all | bytes 16384 | tf_op jit(solution)/shard_map/all_to_all | solution.py:47
  217.7 1.0 copy.54
  (89 shorter events, 3.9 us)
Async XLA Ops:
  6.5 202.5 %copy-start = (bf16[1024,512]{1,0:T(8,128)(2,1)S(1)}, bf16[1024,512]{1,0:T(8,128)(2,1)}, u32[]{:S(2)}) copy-start(bf16[1024,512]{1,0:T(8,128)(2,1)} %param.22) | copy-start | bytes 3145732
  10.7 30.6 %all-to-all-start = ((bf16[4,1,128,2048]{3,2,1,0:T(8,128)(2,1)}), bf16[4,1,128,2048]{3,2,1,0:T(8,128)(2,1)S(1)}, u32[]{:S(2)}, u32[]{:S(2)}) async-start(bf16[4,1,128,2048]{3,2,1,0:T(8,128)(2,1)} %broadcast_in_dim.26), calls=%async_computation | async-start | bytes 4194304 | tf_op jit(solution)/shard_map/all_to_all | solution.py:47
  15.0 112.9 %all-gather.6.cloned.1.call-start = ((), (), s32[]{:S(2)}) async-start(), calls=%async_computation.3 | async-start | bytes 1179648 | tf_op jit(solution)/shard_map/all_gather | solution.py:29
  41.3 2.1 copy-start.7
  43.4 1.2 copy-start.8
  44.6 1.2 copy-start.9
  46.7 1.6 copy-start.1
  46.7 1.3 copy-start.3
  46.7 1.3 copy-start.5
  48.3 2.2 slice-start
  79.7 110.0 %all-gather.8.cloned.1.call-start = ((), (), s32[]{:S(2)}) async-start(), calls=%async_computation.4 | async-start | bytes 1703936 | tf_op jit(solution)/shard_map/all_gather | solution.py:29
  189.7 3.5 %copy-start.6 = (f32[128]{0:T(128)S(1)}, f32[128]{0:T(128)}, u32[]{:S(2)}) copy-start(f32[128]{0:T(128)} %param.21) | copy-start | bytes 1540
  189.7 3.6 %copy-start.2 = (bf16[1,512,1024]{1,2,0:T(8,128)(2,1)S(1)}, bf16[1,512,1024]{1,2,0:T(8,128)(2,1)}, u32[]{:S(2)}) copy-start(bf16[1,512,1024]{1,2,0:T(8,128)(2,1)} %copy-done.1) | copy-start | bytes 3145732
  209.0 8.5 %copy-start.4 = (f32[512]{0:T(512)S(1)}, f32[512]{0:T(512)}, u32[]{:S(2)}) copy-start(f32[512]{0:T(512)} %param.23) | copy-start | bytes 6148
Sparse Core Ops, SparseCore 0:
  79.8 48.0 all-gather.5
  130.4 59.3 all-gather.7
where the time goes:
time: 227 us; the launch traced here: 226 us
  waiting for transfers between devices  93.2 us (41%)
  blocking collectives  66.4 us (29%)
  matrix products  22.5 us (10%)
  local copies, waits for them, and re-layouts  14.2 us (6%)
  between operations  13.8 us (6%)
  other arithmetic  10.8 us (5%)
  starting transfers between devices  4.34 us (2%)
    all_gather x2, waiting for transfers between devices, entering(): pieces = jax.tree.map(lambda part: lax.all_gather(part, axis), so_far)  66.8 us
    all_gather x4, blocking collectives, entering(): pieces = jax.tree.map(lambda part: lax.all_gather(part, axis), so_far)  43.3 us
    all_to_all x1, waiting for transfers between devices, copy_for_each(): return lax.all_to_all(copies, axis, split_axis=0, concat_axis=0, tiled=True)  26.3 us
    all_to_all x2, blocking collectives, copy_for_each(): return lax.all_to_all(copies, axis, split_axis=0, concat_axis=0, tiled=True)  23.1 us
    dot_general x8, matrix products, advance(): jnp.einsum('shtk,shkv->shtv', lifted_q, carried, precision=precise)  7.12 us
    squeeze x8, local copies, waits for them, and re-layouts, block_pass(): lax.scan(advance, initial, (by_block(query_rows), by_block(incoming_weigh...  6.83 us
  transfers between devices with their start and end apart: 3, of which 3 were waited for; matrix products, arithmetic and copies ran while one was open for 1% of the time, Pallas kernels for 0%

commit v1 on v0

v1 whole, which is shorter than its diff:
```python
import jax
import jax.numpy as jnp
from jax import lax
from jax.experimental import pallas as pl
from jax.experimental.pallas import tpu as pltpu
from jax.sharding import Mesh
from jax.sharding import PartitionSpec as P

D = 2048
KEY = 128
SP = ("sp_0", "sp_1", "sp_2")
SP_TP = ("sp_0", "sp_1", "sp_2", "tp")
MESH = pl.DeviceIdType.MESH
EPS = 1e-06

NZ, NY, NC, NX = 12, 8, 2, 4
NM = NY * NC
T = 128
H = T // 2
NB = 4
W2 = 256
PIECE = 256 // NM
MSG = PIECE + 8

bf16 = jnp.bfloat16
f32 = jnp.float32


def dot(a, b, ca=1, cb=0):
    return lax.dot_general(a, b, (((ca,), (cb,)), ((), ())), preferred_element_type=f32)


def split3(x):
    hi = x.astype(bf16).astype(f32)
    rest = x - hi
    mid = rest.astype(bf16).astype(f32)
    return hi, mid, rest - mid


def decay_rows(row):
    hi, mid, lo = split3(row)
    at = lax.broadcasted_iota(jnp.int32, (8, 128), 0)
    rows = jnp.where(at == 0, hi, jnp.where(at == 1, mid, jnp.where(at == 2, lo, 0.0)))
    return rows.astype(bf16)


def body(
    tokens, ing, wq, wf, wi, wg, slack, sud, hgain, wo, ogain, out,
    xin, G, W, WO, lqA, lk, vv, lqD, gs, ST, PB, DT, DP, BC, O,
    msgA, rA, Pp, zout, rz, rout, SIN, GG, PJ, sqo, sqr,
    ldsem, gsR, grR, gsL, grL, sA, qA, sZ, qZ, sR, qR, hsR, hrR, hsL, hrL, sS, qS,
):
    X = lax.axis_index("tp")
    Z = lax.axis_index("sp_0")
    Y = lax.axis_index("sp_1")
    C = lax.axis_index("sp_2")
    M = Y * NC + C
    right = lax.rem(X + 1, NX)
    left = lax.rem(X + NX - 1, NX)
    opp = lax.rem(X + 2, NX)

    def member(m):
        return {"sp_1": m // NC, "sp_2": lax.rem(m, NC)}

    ld_tok = pltpu.make_async_copy(tokens.at[0], xin, ldsem.at[0])
    ld_tok.start()
    loads = [pltpu.make_async_copy(w, W.at[i], ldsem.at[1 + i]) for i, w in enumerate((wq, wf, wi, wg))]
    ld_wo = pltpu.make_async_copy(wo, WO, ldsem.at[5])
    for c in loads:
        c.start()
    ld_wo.start()

    barrier = pltpu.get_barrier_semaphore()
    for dx in range(1, NX):
        pl.semaphore_signal(barrier, inc=1, device_id={"tp": lax.rem(X + dx, NX)}, device_id_type=MESH)
    for dm in range(1, NM):
        pl.semaphore_signal(barrier, inc=1, device_id=member(lax.rem(M + dm, NM)), device_id_type=MESH)
    for dz in range(1, NZ):
        pl.semaphore_signal(barrier, inc=1, device_id={"sp_0": lax.rem(Z + dz, NZ)}, device_id_type=MESH)

    ld_tok.wait()

    def norm_rows(i, _):
        rows = xin[pl.ds(pl.multiple_of(i * 16, 16), 16), :].astype(f32)
        rows = rows * lax.rsqrt(jnp.mean(rows * rows, axis=1, keepdims=True) + EPS) * ing[...]
        G[X, i // 4, pl.ds(pl.multiple_of(lax.rem(i, 4) * 16, 16), 16), :] = rows.astype(bf16)
        return 0

    lax.fori_loop(0, T // 16, norm_rows, 0)
    pl.semaphore_wait(barrier, (NX - 1) + (NM - 1) + (NZ - 1))

    def to_right(who, half, slot):
        return pltpu.make_async_remote_copy(
            G.at[who, half], G.at[who, half], gsR.at[slot], grR.at[slot], device_id={"tp": right}, device_id_type=MESH
        )

    def to_left(who, half, slot):
        return pltpu.make_async_remote_copy(
            G.at[who, half], G.at[who, half], gsL.at[slot], grL.at[slot], device_id={"tp": left}, device_id_type=MESH
        )

    to_right(X, 0, 0).start()
    to_left(X, 1, 0).start()
    to_right(X, 1, 1).start()
    to_left(X, 0, 1).start()

    t_at = lax.broadcasted_iota(jnp.int32, (T, T), 0)
    s_at = lax.broadcasted_iota(jnp.int32, (T, T), 1)
    causal = s_at <= t_at
    tri = causal.astype(f32).astype(bf16)
    for b in range(NB):
        for h in range(2):
            line = jnp.broadcast_to(sud[h : h + 1, b * T : (b + 1) * T], (T, T))
            total = jnp.sum(jnp.where(causal, line, 0.0), axis=1, keepdims=True)
            BC[b, h] = jnp.broadcast_to(total, (T, T))

    for c in loads:
        c.wait()

    def block(b):
        x = G[b].reshape(T, D)
        f_raw = dot(x, W[1]).astype(bf16).astype(f32)
        i_raw = dot(x, W[2]).astype(bf16)
        vv[b] = i_raw
        w = slack[...] * jax.nn.sigmoid(-f_raw)
        a = jnp.log1p(-w)
        a_hi = a.astype(bf16)
        a_lo = (a - a_hi.astype(f32)).astype(bf16)
        A = dot(tri, a_hi) + dot(tri, a_lo)
        lk[b] = (w * jnp.exp(-A)).astype(bf16)
        for h in range(2):
            cols = slice(h * 128, (h + 1) * 128)
            reach = A[:, cols] + BC[b, h]
            end = reach[T - 1 : T, :]
            DT[b, h : h + 1, :] = end
            wk = (w[:, cols] * jnp.exp(end - reach)).astype(bf16)
            ST[b, h] = dot(i_raw[:, cols], wk, 0, 0)
        q_raw = dot(x, W[0]).astype(bf16).astype(f32) * KEY ** (-0.5)
        q_in = q_raw * jnp.exp(A)
        lqA[b] = q_in.astype(bf16)
        for h in range(2):
            cols = slice(h * 128, (h + 1) * 128)
            lqD[b, :, cols] = q_in[:, cols] * jnp.exp(BC[b, h])
        g_raw = dot(x, W[3]).astype(bf16).astype(f32)
        silu = g_raw * jax.nn.sigmoid(g_raw)
        for h in range(2):
            cols = slice(h * 128, (h + 1) * 128)
            gs[b, :, cols] = silu[:, cols] * hgain[...]

    def arrive(i, _):
        @pl.when(i == 1)
        def _():
            to_right(X, 0, 0).wait_recv()
            to_right(left, 0, 2).start()
            to_left(X, 1, 0).wait_recv()
            to_left(right, 1, 2).start()
            to_right(X, 1, 1).wait_recv()
            to_left(X, 0, 1).wait_recv()

        @pl.when(i == 3)
        def _():
            to_right(left, 0, 2).wait_recv()
            to_left(right, 1, 2).wait_recv()

        block(lax.rem(X + 3 * i + 3 * (i // 2) + 2 * (i // 3), NX))
        return 0

    lax.fori_loop(0, NB, arrive, 0)

    finals, totals = [], []
    for h in range(2):
        state = jnp.zeros((128, 128), f32)
        reach = jnp.zeros((1, 128), f32)
        for b in range(NB):
            PB[b, h] = state.astype(bf16)
            DP[b, h : h + 1, :] = reach
            step = DT[b, h : h + 1, :]
            state = jnp.exp(step) * state + ST[b, h]
            reach = reach + step
        finals.append(state)
        totals.append(reach)
    for h in range(2):
        rows = decay_rows(totals[h])
        for j in range(NM // 2):
            m = h * (NM // 2) + j
            msgA[m, 0:PIECE, :] = finals[h][j * PIECE : (j + 1) * PIECE, :].astype(bf16)
            msgA[m, PIECE:MSG, :] = rows

    far_first = sorted(range(1, NM), key=lambda d: -min(d // 2, NY - d // 2))

    def piece_to(dm):
        m = lax.rem(M + dm, NM)
        return pltpu.make_async_remote_copy(
            msgA.at[m], rA.at[M], sA.at[dm], qA.at[dm], device_id=member(m), device_id_type=MESH
        )

    for dm in far_first:
        piece_to(dm).start()
    rA[M] = msgA[M]

    def inner(b, _):
        for h in range(2):
            cols = slice(h * 128, (h + 1) * 128)
            bc = BC[b, h]
            scores = dot(lqA[b, :, cols], lk[b, :, cols], 1, 1)
            scores = scores * jnp.exp(jnp.where(causal, bc - bc.T, -1e30))
            scores = jnp.where(causal, scores, 0.0)
            q_in = lqD[b, :, cols]
            O[b, :, cols] = dot(scores.astype(bf16), vv[b, :, cols]) + dot(q_in.astype(bf16), PB[b, h], 1, 1)
            lqA[b, :, cols] = (q_in * jnp.exp(DP[b, h : h + 1, :])).astype(bf16)
        return 0

    lax.fori_loop(0, NB, inner, 0)

    for dm in range(1, NM):
        piece_to(dm).wait_recv()

    def decay_of(rows):
        part = rows[PIECE:MSG, :].astype(f32)
        return part[0:1, :] + part[1:2, :] + part[2:3, :]

    state = jnp.zeros((PIECE, 128), f32)
    reach = jnp.zeros((1, 128), f32)
    reaches = []
    for m in range(NM):
        rows = rA[m]
        Pp[m] = state
        reaches.append(reach)
        step = decay_of(rows)
        state = jnp.exp(step) * state + rows[0:PIECE, :].astype(f32)
        reach = reach + step
    zout[0:PIECE, :] = state.astype(bf16)
    zout[PIECE:MSG, :] = decay_rows(reach)

    def row_to(z):
        return pltpu.make_async_remote_copy(
            zout, rz.at[Z], sZ.at[z], qZ.at[Z], device_id={"sp_0": z}, device_id_type=MESH
        )

    def row_from(z):
        return pltpu.make_async_remote_copy(
            zout, rz.at[z], sZ.at[z], qZ.at[z], device_id={"sp_0": z}, device_id_type=MESH
        )

    def send_row(z, _):
        row_to(z).start()
        return 0

    lax.fori_loop(Z + 1, NZ, send_row, 0)

    def take_row(z, before):
        row_from(z).wait_recv()
        rows = rz[z]
        return jnp.exp(decay_of(rows)) * before + rows[0:PIECE, :].astype(f32)

    before = lax.fori_loop(0, Z, take_row, jnp.zeros((PIECE, 128), f32))
    for m in range(NM):
        rout[m] = (jnp.exp(reaches[m]) * before + Pp[m]).astype(bf16)

    def back_to(dm):
        m = lax.rem(M + dm, NM)
        return pltpu.make_async_remote_copy(
            rout.at[m], SIN.at[M], sR.at[dm], qR.at[dm], device_id=member(m), device_id_type=MESH
        )

    for dm in far_first:
        back_to(dm).start()
    SIN[M] = rout[M]
    for dm in range(1, NM):
        back_to(dm).wait_recv()

    def h_right(who, r, half, slot):
        return pltpu.make_async_remote_copy(
            GG.at[who, r, half], GG.at[who, r, half], hsR.at[r, slot], hrR.at[r, slot],
            device_id={"tp": right}, device_id_type=MESH,
        )

    def h_left(who, r, half, slot):
        return pltpu.make_async_remote_copy(
            GG.at[who, r, half], GG.at[who, r, half], hsL.at[r, slot], hrL.at[r, slot],
            device_id={"tp": left}, device_id_type=MESH,
        )

    def readout(r, _):
        parts = []
        for h in range(2):
            cols = slice(h * 128, (h + 1) * 128)
            carried = SIN[h * 8 : (h + 1) * 8].reshape(128, 128)
            o = O[r, :, cols] + dot(lqA[r, :, cols], carried, 1, 1)
            o = o * lax.rsqrt(jnp.mean(o * o, axis=1, keepdims=True) + EPS)
            parts.append(o * gs[r, :, cols])
        gated = jnp.concatenate(parts, axis=1).astype(bf16)
        GG[X, r] = gated.reshape(2, H, W2)
        h_right(X, r, 0, 0).start()
        h_left(X, r, 1, 0).start()
        h_right(X, r, 1, 1).start()
        h_left(X, r, 0, 1).start()
        return 0

    lax.fori_loop(0, NB, readout, 0)
    ld_wo.wait()

    def forward(r):
        h_right(X, r, 0, 0).wait_recv()
        h_right(left, r, 0, 2).start()
        h_left(X, r, 1, 0).wait_recv()
        h_left(right, r, 1, 2).start()

    def square_to(dx, r):
        return pltpu.make_async_remote_copy(
            sqo.at[r], sqr.at[dx - 1, r], sS.at[dx - 1, r], qS.at[dx - 1, r],
            device_id={"tp": lax.rem(X + dx, NX)}, device_id_type=MESH,
        )

    def project(r, _):
        @pl.when(r < NB - 1)
        def _():
            forward(r + 1)

        h_right(X, r, 1, 1).wait_recv()
        h_left(X, r, 0, 1).wait_recv()
        h_right(left, r, 0, 2).wait_recv()
        h_left(right, r, 1, 2).wait_recv()
        acc = dot(GG[0, r].reshape(T, W2), WO[0:W2, :])
        for j in range(1, NX):
            acc = acc + dot(GG[j, r].reshape(T, W2), WO[j * W2 : (j + 1) * W2, :])
        PJ[r] = acc
        sq = acc * acc
        sq_hi = sq.astype(bf16)
        sq_lo = (sq - sq_hi.astype(f32)).astype(bf16)
        ones = jnp.ones((8, 512), f32).astype(bf16)
        sqo[r] = dot(ones, sq_hi, 1, 1) + dot(ones, sq_lo, 1, 1)
        for dx in (2, 1, 3):
            square_to(dx, r).start()
        return 0

    forward(0)
    lax.fori_loop(0, NB, project, 0)

    def finish(r, _):
        for dx in (1, 2, 3):
            square_to(dx, r).wait_recv()
        total = sqo[r] + sqr[0, r] + sqr[1, r] + sqr[2, r]
        scale = lax.rsqrt(total[0:1, :] / D + EPS)
        scale = jnp.broadcast_to(scale, (T, T)).T
        for j in range(4):
            cols = slice(j * 128, (j + 1) * 128)
            out[0, pl.ds(pl.multiple_of(r * T, T), T), cols] = (
                PJ[r, :, cols] * scale * ogain[:, cols]
            ).astype(bf16)
        return 0

    lax.fori_loop(0, NB, finish, 0)

    to_right(X, 0, 0).wait_send()
    to_right(X, 1, 1).wait_send()
    to_right(left, 0, 2).wait_send()
    to_left(X, 1, 0).wait_send()
    to_left(X, 0, 1).wait_send()
    to_left(right, 1, 2).wait_send()
    for dm in range(1, NM):
        piece_to(dm).wait_send()
        back_to(dm).wait_send()

    def row_left(z, _):
        row_to(z).wait_send()
        return 0

    lax.fori_loop(Z + 1, NZ, row_left, 0)

    def rest(r, _):
        h_right(X, r, 0, 0).wait_send()
        h_right(X, r, 1, 1).wait_send()
        h_right(left, r, 0, 2).wait_send()
        h_left(X, r, 1, 0).wait_send()
        h_left(X, r, 0, 1).wait_send()
        h_left(right, r, 1, 2).wait_send()
        for dx in (1, 2, 3):
            square_to(dx, r).wait_send()
        return 0

    lax.fori_loop(0, NB, rest, 0)


def shards(tokens, ing, wq, wf, wi, wg, slack, sud, hgain, wo, ogain):
    vm = pl.BlockSpec(memory_space=pltpu.VMEM)
    hb = pl.BlockSpec(memory_space=pl.ANY)
    dma = pltpu.SemaphoreType.DMA
    V = pltpu.VMEM
    return pl.pallas_call(
        body,
        name="layer",
        out_shape=jax.ShapeDtypeStruct((1, 512, 512), bf16),
        in_specs=[hb, vm, hb, hb, hb, hb, vm, vm, vm, hb, vm],
        out_specs=vm,
        scratch_shapes=[
            V((T, D), bf16),
            V((NX, 2, H, D), bf16),
            V((4, D, W2), bf16),
            V((1024, 512), bf16),
            V((NB, T, W2), bf16),
            V((NB, T, W2), bf16),
            V((NB, T, W2), bf16),
            V((NB, T, W2), f32),
            V((NB, T, W2), f32),
            V((NB, 2, 128, 128), f32),
            V((NB, 2, 128, 128), bf16),
            V((NB, 2, 128), f32),
            V((NB, 2, 128), f32),
            V((NB, 2, T, T), f32),
            V((NB, T, W2), f32),
            V((NM, MSG, 128), bf16),
            V((NM, MSG, 128), bf16),
            V((NM, PIECE, 128), f32),
            V((MSG, 128), bf16),
            V((NZ, MSG, 128), bf16),
            V((NM, PIECE, 128), bf16),
            V((NM, PIECE, 128), bf16),
            V((NX, NB, 2, H, W2), bf16),
            V((NB, T, 512), f32),
            V((NB, 8, 128), f32),
            V((3, NB, 8, 128), f32),
            dma((6,)),
            dma((3,)), dma((3,)), dma((3,)), dma((3,)),
            dma((NM,)), dma((NM,)),
            dma((NZ,)), dma((NZ,)),
            dma((NM,)), dma((NM,)),
            dma((NB, 3)), dma((NB, 3)), dma((NB, 3)), dma((NB, 3)),
            dma((3, NB)), dma((3, NB)),
        ],
        compiler_params=pltpu.CompilerParams(
            collective_id=0, has_side_effects=True, vmem_limit_bytes=60 * 1024 * 1024
        ),
    )(
        tokens,
        ing.reshape(1, D),
        wq, wf, wi, wg,
        slack.reshape(1, W2),
        sud[0].T,
        hgain.reshape(1, 128),
        wo,
        ogain.reshape(1, 512),
    )


def solution(mesh):
    torus = Mesh(mesh.devices.reshape(NZ, NY, NC, NX), ("sp_0", "sp_1", "sp_2", "tp"))
    in_specs = (
        P(None, SP_TP, None),
        P(),
        P(None, "tp"),
        P(None, "tp"),
        P(None, "tp"),
        P(None, "tp"),
        P("tp"),
        P(None, SP, "tp"),
        P(),
        P(None, "tp"),
        P("tp"),
    )
    out_specs = P(None, SP, "tp")
    return jax.shard_map(shards, mesh=torus, in_specs=in_specs, out_specs=out_specs, check_vma=False)
```

time: 227 us -> 71.4 us (0.31)
  the two profiles are of different devices: /device:TPU:8 before, /device:TPU:64 now
where the time goes in v1:
time: 71.4 us; the launch traced here: 71.2 us
  Pallas kernels  69.3 us (97%)
  local copies, waits for them, and re-layouts  1.87 us (3%)
    pallas_call x1, Pallas kernels, shards(): pl.pallas_call(body, name='layer', out_shape=jax.ShapeDtypeStruct((1, 512...  69.3 us
    unnamed x1, local copies, waits for them, and re-layouts  1.87 us

profile of v1, /device:TPU:64, one launch (start us, length us, event | category | flops | bytes accessed | tf_op | source)
XLA Modules:
  0.0 71.2 jit_solution(16588476907077741766)
XLA Ops:
  0.0 69.3 %layer.1 = bf16[1,512,512]{2,1,0:T(8,128)(2,1)} custom-call(bf16[1,128,2048]{2,1,0:T(8,128)(2,1)} %tokens.1, f32[1,2048]{1,0:T(1,128)} %bitcast.7, bf16[2048,256]{1,0:T(8,128)(2,1)} %wq.1, bf16[2048,256]{1,0:T(8,128)(2,1)} %wf.1, bf16[2048,256]{1,0:T(8,128)(2,1)} %wi.1, bf16[2048,256]{1,0:T(8,128)(2,1)} %wg.1, f32[1,256]{1,0:T(1,128)} %bitcast.10, ...), custom_call_target="tpu_custom_call" | custom-call | tf_op jit(solution)/shard_map/layer/pallas_call | solution.py:390
  69.3 1.9 %copy.13 = bf16[1,512,512]{2,1,0:T(8,128)(2,1)} copy(bf16[1,512,512]{2,1,0:T(8,128)(2,1)} %layer.1) | data formatting | bytes 1048576

commit v2 on v1

--- a/solution.py
+++ b/solution.py
@@ -17,6 +17,8 @@
 NM = NY * NC
 T = 128
 H = T // 2
+Q = T // 4
+OUTER = (0, 3, 1, 2)
 NB = 4
 W2 = 256
 PIECE = 256 // NM
@@ -45,10 +47,11 @@
 
 
 def body(
-    tokens, ing, wq, wf, wi, wg, slack, sud, hgain, wo, ogain, out,
-    xin, G, W, WO, lqA, lk, vv, lqD, gs, ST, PB, DT, DP, BC, O,
+    tokens, ing_in, wq, wf, wi, wg, slack_in, sud_in, hgain_in, wo, ogain_in, out,
+    ing, slack, sud, hgain, ogain,
+    xin, G, W, WO, lqA, lk, vv, lqD, gs, ST, PB, DT, DP, BC, AA, O,
     msgA, rA, Pp, zout, rz, rout, SIN, GG, PJ, sqo, sqr,
-    ldsem, gsR, grR, gsL, grL, sA, qA, sZ, qZ, sR, qR, hsR, hrR, hsL, hrL, sS, qS,
+    tksem, smsem, ldsem, gsR, grR, gsL, grL, sA, qA, sZ, qZ, sR, qR, hsR, hrR, hsL, hrL, sS, qS, rdyM, rdyZ,
 ):
     X = lax.axis_index("tp")
     Z = lax.axis_index("sp_0")
@@ -62,10 +65,26 @@
     def member(m):
         return {"sp_1": m // NC, "sp_2": lax.rem(m, NC)}
 
-    ld_tok = pltpu.make_async_copy(tokens.at[0], xin, ldsem.at[0])
-    ld_tok.start()
-    loads = [pltpu.make_async_copy(w, W.at[i], ldsem.at[1 + i]) for i, w in enumerate((wq, wf, wi, wg))]
-    ld_wo = pltpu.make_async_copy(wo, WO, ldsem.at[5])
+    late = jnp.where(Z == 0, NM - 1, 0)
+    mine = lax.rem(M + late, NM)
+
+    def load_rows(k):
+        rows = pl.ds(k * Q, Q)
+        return pltpu.make_async_copy(tokens.at[0, rows], xin.at[rows], tksem.at[k])
+
+    small = [
+        pltpu.make_async_copy(a, b, smsem.at[i])
+        for i, (a, b) in enumerate(
+            ((ing_in, ing), (slack_in, slack), (sud_in, sud), (hgain_in, hgain), (ogain_in, ogain))
+        )
+    ]
+    loads = [pltpu.make_async_copy(w, W.at[i], ldsem.at[i]) for i, w in enumerate((wq, wf, wi, wg))]
+    ld_wo = pltpu.make_async_copy(wo, WO, ldsem.at[4])
+    small[0].start()
+    for k in OUTER:
+        load_rows(k).start()
+    for c in small[1:]:
+        c.start()
     for c in loads:
         c.start()
     ld_wo.start()
@@ -73,36 +92,72 @@
     barrier = pltpu.get_barrier_semaphore()
     for dx in range(1, NX):
         pl.semaphore_signal(barrier, inc=1, device_id={"tp": lax.rem(X + dx, NX)}, device_id_type=MESH)
-    for dm in range(1, NM):
-        pl.semaphore_signal(barrier, inc=1, device_id=member(lax.rem(M + dm, NM)), device_id_type=MESH)
-    for dz in range(1, NZ):
-        pl.semaphore_signal(barrier, inc=1, device_id={"sp_0": lax.rem(Z + dz, NZ)}, device_id_type=MESH)
-
-    ld_tok.wait()
-
-    def norm_rows(i, _):
-        rows = xin[pl.ds(pl.multiple_of(i * 16, 16), 16), :].astype(f32)
-        rows = rows * lax.rsqrt(jnp.mean(rows * rows, axis=1, keepdims=True) + EPS) * ing[...]
-        G[X, i // 4, pl.ds(pl.multiple_of(lax.rem(i, 4) * 16, 16), 16), :] = rows.astype(bf16)
-        return 0
-
-    lax.fori_loop(0, T // 16, norm_rows, 0)
-    pl.semaphore_wait(barrier, (NX - 1) + (NM - 1) + (NZ - 1))
-
-    def to_right(who, half, slot):
-        return pltpu.make_async_remote_copy(
-            G.at[who, half], G.at[who, half], gsR.at[slot], grR.at[slot], device_id={"tp": right}, device_id_type=MESH
-        )
-
-    def to_left(who, half, slot):
-        return pltpu.make_async_remote_copy(
-            G.at[who, half], G.at[who, half], gsL.at[slot], grL.at[slot], device_id={"tp": left}, device_id_type=MESH
-        )
-
+
+    def greet_row(k, _):
+        pl.semaphore_signal(barrier, inc=1, device_id=member(lax.rem(k + NM - late, NM)), device_id_type=MESH)
+        return 0
+
+    def greet_line(z, _):
+        pl.semaphore_signal(barrier, inc=1, device_id={"sp_0": z}, device_id_type=MESH)
+        return 0
+
+    lax.fori_loop(mine + 1, NM, greet_row, 0)
+    lax.fori_loop(Z + 1, NZ, greet_line, 0)
+
+    small[0].wait()
+
+    def norm_rows(k):
+        def some(i, _):
+            at = pl.ds(pl.multiple_of(k * Q + i * 16, 16), 16)
+            rows = xin[at, :].astype(f32)
+            rows = rows * lax.rsqrt(jnp.mean(rows * rows, axis=1, keepdims=True) + EPS) * ing[...]
+            G[X, k, pl.ds(pl.multiple_of(i * 16, 16), 16), :] = rows.astype(bf16)
+            return 0
+
+        lax.fori_loop(0, Q // 16, some, 0)
+
+    def to_right(who, k, slot):
+        return pltpu.make_async_remote_copy(
+            G.at[who, k], G.at[who, k], gsR.at[slot], grR.at[slot], device_id={"tp": right}, device_id_type=MESH
+        )
+
+    def to_left(who, k, slot):
+        return pltpu.make_async_remote_copy(
+            G.at[who, k], G.at[who, k], gsL.at[slot], grL.at[slot], device_id={"tp": left}, device_id_type=MESH
+        )
+
+    load_rows(0).wait()
+    norm_rows(0)
+    with jax.named_scope("barrier"):
+        pl.semaphore_wait(barrier, (NX - 1) + mine + Z)
     to_right(X, 0, 0).start()
-    to_left(X, 1, 0).start()
+    load_rows(3).wait()
+    norm_rows(3)
+    to_left(X, 3, 3).start()
+    load_rows(1).wait()
+    norm_rows(1)
     to_right(X, 1, 1).start()
-    to_left(X, 0, 1).start()
+    load_rows(2).wait()
+    norm_rows(2)
+    to_left(X, 2, 2).start()
+    to_right(X, 2, 2).start()
+    to_left(X, 1, 1).start()
+    to_right(X, 3, 3).start()
+    to_left(X, 0, 0).start()
+
+    def ready_row(k, _):
+        pl.semaphore_signal(rdyM, inc=1, device_id=member(lax.rem(k + NM - late, NM)), device_id_type=MESH)
+        return 0
+
+    def ready_line(z, _):
+        pl.semaphore_signal(rdyZ, inc=1, device_id={"sp_0": z}, device_id_type=MESH)
+        return 0
+
+    lax.fori_loop(0, mine, ready_row, 0)
+    lax.fori_loop(0, Z, ready_line, 0)
+
+    for c in small[1:]:
+        c.wait()
 
     t_at = lax.broadcasted_iota(jnp.int32, (T, T), 0)
     s_at = lax.broadcasted_iota(jnp.int32, (T, T), 1)
@@ -114,10 +169,11 @@
             total = jnp.sum(jnp.where(causal, line, 0.0), axis=1, keepdims=True)
             BC[b, h] = jnp.broadcast_to(total, (T, T))
 
-    for c in loads:
-        c.wait()
-
-    def block(b):
+    with jax.named_scope("wload"):
+        for c in loads:
+            c.wait()
+
+    def block_state(b):
         x = G[b].reshape(T, D)
         f_raw = dot(x, W[1]).astype(bf16).astype(f32)
         i_raw = dot(x, W[2]).astype(bf16)
@@ -127,6 +183,7 @@
         a_hi = a.astype(bf16)
         a_lo = (a - a_hi.astype(f32)).astype(bf16)
         A = dot(tri, a_hi) + dot(tri, a_lo)
+        AA[b] = A
         lk[b] = (w * jnp.exp(-A)).astype(bf16)
         for h in range(2):
             cols = slice(h * 128, (h + 1) * 128)
@@ -135,8 +192,11 @@
             DT[b, h : h + 1, :] = end
             wk = (w[:, cols] * jnp.exp(end - reach)).astype(bf16)
             ST[b, h] = dot(i_raw[:, cols], wk, 0, 0)
+
+    def block_rest(b):
+        x = G[b].reshape(T, D)
         q_raw = dot(x, W[0]).astype(bf16).astype(f32) * KEY ** (-0.5)
-        q_in = q_raw * jnp.exp(A)
+        q_in = q_raw * jnp.exp(AA[b])
         lqA[b] = q_in.astype(bf16)
         for h in range(2):
             cols = slice(h * 128, (h + 1) * 128)
@@ -150,19 +210,37 @@
     def arrive(i, _):
         @pl.when(i == 1)
         def _():
-            to_right(X, 0, 0).wait_recv()
-            to_right(left, 0, 2).start()
-            to_left(X, 1, 0).wait_recv()
-            to_left(right, 1, 2).start()
-            to_right(X, 1, 1).wait_recv()
-            to_left(X, 0, 1).wait_recv()
+            with jax.named_scope("g1"):
+                to_right(X, 0, 0).wait_recv()
+                to_right(left, 0, 4).start()
+                to_left(X, 3, 3).wait_recv()
+                to_left(right, 3, 4).start()
+                to_right(X, 1, 1).wait_recv()
+                to_right(left, 1, 5).start()
+                to_left(X, 2, 2).wait_recv()
+                to_left(right, 2, 5).start()
+            with jax.named_scope("g2"):
+                for k in (2, 3):
+                    to_right(X, k, k).wait_recv()
+                    to_left(X, 3 - k, 3 - k).wait_recv()
 
         @pl.when(i == 3)
         def _():
-            to_right(left, 0, 2).wait_recv()
-            to_left(right, 1, 2).wait_recv()
-
-        block(lax.rem(X + 3 * i + 3 * (i // 2) + 2 * (i // 3), NX))
+            with jax.named_scope("g3"):
+                to_right(left, 0, 4).wait_recv()
+                to_left(right, 3, 4).wait_recv()
+                to_right(left, 1, 5).wait_recv()
+                to_left(right, 2, 5).wait_recv()
+
+        b = lax.rem(X + 3 * i + 3 * (i // 2) + 2 * (i // 3), NX)
+        with jax.named_scope("state"):
+            block_state(b)
+
+        @pl.when(i < 3)
+        def _():
+            with jax.named_scope("rest"):
+                block_rest(b)
+
         return 0
 
     lax.fori_loop(0, NB, arrive, 0)
@@ -194,9 +272,16 @@
             msgA.at[m], rA.at[M], sA.at[dm], qA.at[dm], device_id=member(m), device_id_type=MESH
         )
 
+    @pl.when(mine < NM - 1)
+    def _():
+        pl.semaphore_wait(rdyM, NM - 1 - mine)
+
     for dm in far_first:
         piece_to(dm).start()
     rA[M] = msgA[M]
+
+    with jax.named_scope("rest3"):
+        block_rest(opp)
 
     def inner(b, _):
         for h in range(2):
@@ -210,10 +295,12 @@
             lqA[b, :, cols] = (q_in * jnp.exp(DP[b, h : h + 1, :])).astype(bf16)
         return 0
 
-    lax.fori_loop(0, NB, inner, 0)
-
-    for dm in range(1, NM):
-        piece_to(dm).wait_recv()
+    with jax.named_scope("inner"):
+        lax.fori_loop(0, NB, inner, 0)
+
+    with jax.named_scope("rswait"):
+        for dm in range(1, NM):
+            piece_to(dm).wait_recv()
 
     def decay_of(rows):
         part = rows[PIECE:MSG, :].astype(f32)
@@ -246,6 +333,10 @@
         row_to(z).start()
         return 0
 
+    @pl.when(Z < NZ - 1)
+    def _():
+        pl.semaphore_wait(rdyZ, NZ - 1 - Z)
+
     lax.fori_loop(Z + 1, NZ, send_row, 0)
 
     def take_row(z, before):
@@ -253,7 +344,8 @@
         rows = rz[z]
         return jnp.exp(decay_of(rows)) * before + rows[0:PIECE, :].astype(f32)
 
-    before = lax.fori_loop(0, Z, take_row, jnp.zeros((PIECE, 128), f32))
+    with jax.named_scope("zwait"):
+        before = lax.fori_loop(0, Z, take_row, jnp.zeros((PIECE, 128), f32))
     for m in range(NM):
         rout[m] = (jnp.exp(reaches[m]) * before + Pp[m]).astype(bf16)
 
@@ -266,8 +358,9 @@
     for dm in far_first:
         back_to(dm).start()
     SIN[M] = rout[M]
-    for dm in range(1, NM):
-        back_to(dm).wait_recv()
+    with jax.named_scope("backwait"):
+        for dm in range(1, NM):
+            back_to(dm).wait_recv()
 
     def h_right(who, r, half, slot):
         return pltpu.make_async_remote_copy(
@@ -297,8 +390,9 @@
         h_left(X, r, 0, 1).start()
         return 0
 
-    lax.fori_loop(0, NB, readout, 0)
-    ld_wo.wait()
+    with jax.named_scope("readout"):
+        lax.fori_loop(0, NB, readout, 0)
+        ld_wo.wait()
 
     def forward(r):
         h_right(X, r, 0, 0).wait_recv()
@@ -315,12 +409,14 @@
     def project(r, _):
         @pl.when(r < NB - 1)
         def _():
-            forward(r + 1)
-
-        h_right(X, r, 1, 1).wait_recv()
-        h_left(X, r, 0, 1).wait_recv()
-        h_right(left, r, 0, 2).wait_recv()
-        h_left(right, r, 1, 2).wait_recv()
+            with jax.named_scope("hfwd"):
+                forward(r + 1)
+
+        with jax.named_scope("hwait"):
+            h_right(X, r, 1, 1).wait_recv()
+            h_left(X, r, 0, 1).wait_recv()
+            h_right(left, r, 0, 2).wait_recv()
+            h_left(right, r, 1, 2).wait_recv()
         acc = dot(GG[0, r].reshape(T, W2), WO[0:W2, :])
         for j in range(1, NX):
             acc = acc + dot(GG[j, r].reshape(T, W2), WO[j * W2 : (j + 1) * W2, :])
@@ -334,12 +430,14 @@
             square_to(dx, r).start()
         return 0
 
-    forward(0)
+    with jax.named_scope("hfwd0"):
+        forward(0)
     lax.fori_loop(0, NB, project, 0)
 
     def finish(r, _):
-        for dx in (1, 2, 3):
-            square_to(dx, r).wait_recv()
+        with jax.named_scope("sqwait"):
+            for dx in (1, 2, 3):
+                square_to(dx, r).wait_recv()
         total = sqo[r] + sqr[0, r] + sqr[1, r] + sqr[2, r]
         scale = lax.rsqrt(total[0:1, :] / D + EPS)
         scale = jnp.broadcast_to(scale, (T, T)).T
@@ -352,12 +450,12 @@
 
     lax.fori_loop(0, NB, finish, 0)
 
-    to_right(X, 0, 0).wait_send()
-    to_right(X, 1, 1).wait_send()
-    to_right(left, 0, 2).wait_send()
-    to_left(X, 1, 0).wait_send()
-    to_left(X, 0, 1).wait_send()
-    to_left(right, 1, 2).wait_send()
+    for k in range(4):
+        to_right(X, k, k).wait_send()
+        to_left(X, k, k).wait_send()
+    for k in range(2):
+        to_right(left, k, 4 + k).wait_send()
+        to_left(right, 3 - k, 4 + k).wait_send()
     for dm in range(1, NM):
         piece_to(dm).wait_send()
         back_to(dm).wait_send()
@@ -384,18 +482,19 @@
 
 def shards(tokens, ing, wq, wf, wi, wg, slack, sud, hgain, wo, ogain):
     vm = pl.BlockSpec(memory_space=pltpu.VMEM)
-    hb = pl.BlockSpec(memory_space=pl.ANY)
+    hb = pl.BlockSpec(memory_space=pltpu.HBM)
     dma = pltpu.SemaphoreType.DMA
     V = pltpu.VMEM
     return pl.pallas_call(
         body,
         name="layer",
         out_shape=jax.ShapeDtypeStruct((1, 512, 512), bf16),
-        in_specs=[hb, vm, hb, hb, hb, hb, vm, vm, vm, hb, vm],
+        in_specs=[hb] * 11,
         out_specs=vm,
         scratch_shapes=[
+            V((1, D), f32), V((1, W2), f32), V((2, 512), f32), V((1, 128), f32), V((1, 512), f32),
             V((T, D), bf16),
-            V((NX, 2, H, D), bf16),
+            V((NX, 4, Q, D), bf16),
             V((4, D, W2), bf16),
             V((1024, 512), bf16),
             V((NB, T, W2), bf16),
@@ -408,6 +507,7 @@
             V((NB, 2, 128), f32),
             V((NB, 2, 128), f32),
             V((NB, 2, T, T), f32),
+            V((NX, T, W2), f32),
             V((NB, T, W2), f32),
             V((NM, MSG, 128), bf16),
             V((NM, MSG, 128), bf16),
@@ -420,13 +520,14 @@
             V((NB, T, 512), f32),
             V((NB, 8, 128), f32),
             V((3, NB, 8, 128), f32),
-            dma((6,)),
-            dma((3,)), dma((3,)), dma((3,)), dma((3,)),
+            dma((4,)), dma((5,)), dma((5,)),
+            dma((6,)), dma((6,)), dma((6,)), dma((6,)),
             dma((NM,)), dma((NM,)),
             dma((NZ,)), dma((NZ,)),
             dma((NM,)), dma((NM,)),
             dma((NB, 3)), dma((NB, 3)), dma((NB, 3)), dma((NB, 3)),
             dma((3, NB)), dma((3, NB)),
+            pltpu.SemaphoreType.REGULAR, pltpu.SemaphoreType.REGULAR,
         ],
         compiler_params=pltpu.CompilerParams(
             collective_id=0, has_side_effects=True, vmem_limit_bytes=60 * 1024 * 1024

time: 71.4 us -> 61.8 us (0.87)
  the two profiles are of different devices: /device:TPU:64 before, /device:TPU:704 now
where the time goes in v2:
time: 61.8 us; the launch traced here: 61.6 us
  Pallas kernels  59.8 us (97%)
  local copies, waits for them, and re-layouts  1.87 us (3%)
    pallas_call x1, Pallas kernels, shards(): pl.pallas_call(body, name='layer', out_shape=jax.ShapeDtypeStruct((1, 512...  59.8 us
    unnamed x1, local copies, waits for them, and re-layouts  1.87 us

profile of v2, /device:TPU:704, one launch (start us, length us, event | category | flops | bytes accessed | tf_op | source)
XLA Modules:
  0.0 61.6 jit_solution(342961193526187973)
XLA Ops:
  0.0 59.8 %layer.1 = bf16[1,512,512]{2,1,0:T(8,128)(2,1)} custom-call(bf16[1,128,2048]{2,1,0:T(8,128)(2,1)} %tokens.1, f32[1,2048]{1,0:T(1,128)} %bitcast.7, bf16[2048,256]{1,0:T(8,128)(2,1)} %wq.1, bf16[2048,256]{1,0:T(8,128)(2,1)} %wf.1, bf16[2048,256]{1,0:T(8,128)(2,1)} %wi.1, bf16[2048,256]{1,0:T(8,128)(2,1)} %wg.1, f32[1,256]{1,0:T(1,128)} %bitcast.10, ...), custom_call_target="tpu_custom_call" | custom-call | tf_op jit(solution)/shard_map/layer/pallas_call | solution.py:488
  59.8 1.9 %copy.13 = bf16[1,512,512]{2,1,0:T(8,128)(2,1)} copy(bf16[1,512,512]{2,1,0:T(8,128)(2,1)} %layer.1) | data formatting | bytes 1048576

commit v3 on v2

--- a/solution.py
+++ b/solution.py
@@ -21,7 +21,8 @@
 OUTER = (0, 3, 1, 2)
 NB = 4
 W2 = 256
-PIECE = 256 // NM
+NP = NY
+PIECE = 256 // NP
 MSG = PIECE + 8
 
 bf16 = jnp.bfloat16
@@ -68,6 +69,10 @@
     late = jnp.where(Z == 0, NM - 1, 0)
     mine = lax.rem(M + late, NM)
 
+    barrier = pltpu.get_barrier_semaphore()
+    for dx in range(1, NX):
+        pl.semaphore_signal(barrier, inc=1, device_id={"tp": lax.rem(X + dx, NX)}, device_id_type=MESH)
+
     def load_rows(k):
         rows = pl.ds(k * Q, Q)
         return pltpu.make_async_copy(tokens.at[0, rows], xin.at[rows], tksem.at[k])
@@ -89,10 +94,6 @@
         c.start()
     ld_wo.start()
 
-    barrier = pltpu.get_barrier_semaphore()
-    for dx in range(1, NX):
-        pl.semaphore_signal(barrier, inc=1, device_id={"tp": lax.rem(X + dx, NX)}, device_id_type=MESH)
-
     def greet_row(k, _):
         pl.semaphore_signal(barrier, inc=1, device_id=member(lax.rem(k + NM - late, NM)), device_id_type=MESH)
         return 0
@@ -102,7 +103,11 @@
         return 0
 
     lax.fori_loop(mine + 1, NM, greet_row, 0)
-    lax.fori_loop(Z + 1, NZ, greet_line, 0)
+
+    @pl.when(C == 1)
+    def _():
+        lax.fori_loop(Z + 1, NZ, greet_line, 0)
+
 
     small[0].wait()
 
@@ -129,7 +134,7 @@
     load_rows(0).wait()
     norm_rows(0)
     with jax.named_scope("barrier"):
-        pl.semaphore_wait(barrier, (NX - 1) + mine + Z)
+        pl.semaphore_wait(barrier, (NX - 1) + mine + Z * C)
     to_right(X, 0, 0).start()
     load_rows(3).wait()
     norm_rows(3)
@@ -154,7 +159,11 @@
         return 0
 
     lax.fori_loop(0, mine, ready_row, 0)
-    lax.fori_loop(0, Z, ready_line, 0)
+
+    @pl.when(C == 1)
+    def _():
+        lax.fori_loop(0, Z, ready_line, 0)
+
 
     for c in small[1:]:
         c.wait()
@@ -259,26 +268,39 @@
         totals.append(reach)
     for h in range(2):
         rows = decay_rows(totals[h])
-        for j in range(NM // 2):
-            m = h * (NM // 2) + j
-            msgA[m, 0:PIECE, :] = finals[h][j * PIECE : (j + 1) * PIECE, :].astype(bf16)
-            msgA[m, PIECE:MSG, :] = rows
-
-    far_first = sorted(range(1, NM), key=lambda d: -min(d // 2, NY - d // 2))
-
-    def piece_to(dm):
-        m = lax.rem(M + dm, NM)
-        return pltpu.make_async_remote_copy(
-            msgA.at[m], rA.at[M], sA.at[dm], qA.at[dm], device_id=member(m), device_id_type=MESH
+        for j in range(NP // 2):
+            p = h * (NP // 2) + j
+            msgA[p, 0:PIECE, :] = finals[h][j * PIECE : (j + 1) * PIECE, :].astype(bf16)
+            msgA[p, PIECE:MSG, :] = rows
+
+    far_first = sorted(range(NP), key=lambda d: -min(d, NP - d))
+
+    def piece_to(dy):
+        p = lax.rem(Y + dy, NP)
+        at = 2 * dy + 1 - C
+        return pltpu.make_async_remote_copy(
+            msgA.at[p], rA.at[M], sA.at[dy], qA.at[at], device_id={"sp_1": p, "sp_2": 1}, device_id_type=MESH
+        )
+
+    def piece_from(at):
+        return pltpu.make_async_remote_copy(
+            msgA.at[0], rA.at[M], sA.at[0], qA.at[at], device_id={"sp_1": Y, "sp_2": 1}, device_id_type=MESH
         )
 
     @pl.when(mine < NM - 1)
     def _():
         pl.semaphore_wait(rdyM, NM - 1 - mine)
 
-    for dm in far_first:
-        piece_to(dm).start()
-    rA[M] = msgA[M]
+    for dy in far_first[:-1]:
+        piece_to(dy).start()
+
+    @pl.when(C == 0)
+    def _():
+        piece_to(0).start()
+
+    @pl.when(C == 1)
+    def _():
+        rA[M] = msgA[Y]
 
     with jax.named_scope("rest3"):
         block_rest(opp)
@@ -298,27 +320,10 @@
     with jax.named_scope("inner"):
         lax.fori_loop(0, NB, inner, 0)
 
-    with jax.named_scope("rswait"):
-        for dm in range(1, NM):
-            piece_to(dm).wait_recv()
-
     def decay_of(rows):
         part = rows[PIECE:MSG, :].astype(f32)
         return part[0:1, :] + part[1:2, :] + part[2:3, :]
 
-    state = jnp.zeros((PIECE, 128), f32)
-    reach = jnp.zeros((1, 128), f32)
-    reaches = []
-    for m in range(NM):
-        rows = rA[m]
-        Pp[m] = state
-        reaches.append(reach)
-        step = decay_of(rows)
-        state = jnp.exp(step) * state + rows[0:PIECE, :].astype(f32)
-        reach = reach + step
-    zout[0:PIECE, :] = state.astype(bf16)
-    zout[PIECE:MSG, :] = decay_rows(reach)
-
     def row_to(z):
         return pltpu.make_async_remote_copy(
             zout, rz.at[Z], sZ.at[z], qZ.at[Z], device_id={"sp_0": z}, device_id_type=MESH
@@ -332,35 +337,65 @@
     def send_row(z, _):
         row_to(z).start()
         return 0
-
-    @pl.when(Z < NZ - 1)
-    def _():
-        pl.semaphore_wait(rdyZ, NZ - 1 - Z)
-
-    lax.fori_loop(Z + 1, NZ, send_row, 0)
 
     def take_row(z, before):
         row_from(z).wait_recv()
         rows = rz[z]
         return jnp.exp(decay_of(rows)) * before + rows[0:PIECE, :].astype(f32)
 
-    with jax.named_scope("zwait"):
-        before = lax.fori_loop(0, Z, take_row, jnp.zeros((PIECE, 128), f32))
-    for m in range(NM):
-        rout[m] = (jnp.exp(reaches[m]) * before + Pp[m]).astype(bf16)
-
     def back_to(dm):
         m = lax.rem(M + dm, NM)
         return pltpu.make_async_remote_copy(
-            rout.at[m], SIN.at[M], sR.at[dm], qR.at[dm], device_id=member(m), device_id_type=MESH
-        )
-
-    for dm in far_first:
-        back_to(dm).start()
-    SIN[M] = rout[M]
+            rout.at[m], SIN.at[Y], sR.at[dm], qR.at[Y], device_id=member(m), device_id_type=MESH
+        )
+
+    def back_from(dy):
+        p = lax.rem(Y + dy, NP)
+        return pltpu.make_async_remote_copy(
+            rout.at[0], SIN.at[p], sR.at[0], qR.at[p], device_id={"sp_1": p, "sp_2": 1}, device_id_type=MESH
+        )
+
+    back_order = sorted(range(1, NM), key=lambda d: -min(d // 2, NY - d // 2))
+
+    @pl.when(C == 1)
+    def _():
+        with jax.named_scope("rswait"):
+            for at in range(1, NM):
+                piece_from(at).wait_recv()
+
+        state = jnp.zeros((PIECE, 128), f32)
+        reach = jnp.zeros((1, 128), f32)
+        reaches = []
+        for m in range(NM):
+            rows = rA[m]
+            Pp[m] = state
+            reaches.append(reach)
+            step = decay_of(rows)
+            state = jnp.exp(step) * state + rows[0:PIECE, :].astype(f32)
+            reach = reach + step
+        zout[0:PIECE, :] = state.astype(bf16)
+        zout[PIECE:MSG, :] = decay_rows(reach)
+
+        @pl.when(Z < NZ - 1)
+        def _():
+            pl.semaphore_wait(rdyZ, NZ - 1 - Z)
+
+        lax.fori_loop(Z + 1, NZ, send_row, 0)
+        with jax.named_scope("zwait"):
+            before = lax.fori_loop(0, Z, take_row, jnp.zeros((PIECE, 128), f32))
+        for m in range(NM):
+            rout[m] = (jnp.exp(reaches[m]) * before + Pp[m]).astype(bf16)
+        for dm in back_order:
+            back_to(dm).start()
+        SIN[Y] = rout[M]
+
     with jax.named_scope("backwait"):
-        for dm in range(1, NM):
-            back_to(dm).wait_recv()
+        for dy in far_first[:-1]:
+            back_from(dy).wait_recv()
+
+        @pl.when(C == 0)
+        def _():
+            back_from(0).wait_recv()
 
     def h_right(who, r, half, slot):
         return pltpu.make_async_remote_copy(
@@ -378,7 +413,7 @@
         parts = []
         for h in range(2):
             cols = slice(h * 128, (h + 1) * 128)
-            carried = SIN[h * 8 : (h + 1) * 8].reshape(128, 128)
+            carried = SIN[h * (NP // 2) : (h + 1) * (NP // 2)].reshape(128, 128)
             o = O[r, :, cols] + dot(lqA[r, :, cols], carried, 1, 1)
             o = o * lax.rsqrt(jnp.mean(o * o, axis=1, keepdims=True) + EPS)
             parts.append(o * gs[r, :, cols])
@@ -406,20 +441,26 @@
             device_id={"tp": lax.rem(X + dx, NX)}, device_id_type=MESH,
         )
 
-    def project(r, _):
-        @pl.when(r < NB - 1)
-        def _():
-            with jax.named_scope("hfwd"):
-                forward(r + 1)
-
-        with jax.named_scope("hwait"):
+    for r in range(NB):
+        with jax.named_scope("hfwd"):
+            forward(r)
+
+    def near(r, _):
+        with jax.named_scope("hnear"):
             h_right(X, r, 1, 1).wait_recv()
             h_left(X, r, 0, 1).wait_recv()
+        acc = dot(GG[X, r].reshape(T, W2), WO[X])
+        acc = acc + dot(GG[left, r].reshape(T, W2), WO[left])
+        PJ[r] = acc + dot(GG[right, r].reshape(T, W2), WO[right])
+        return 0
+
+    lax.fori_loop(0, NB, near, 0)
+
+    def far(r, _):
+        with jax.named_scope("hfar"):
             h_right(left, r, 0, 2).wait_recv()
             h_left(right, r, 1, 2).wait_recv()
-        acc = dot(GG[0, r].reshape(T, W2), WO[0:W2, :])
-        for j in range(1, NX):
-            acc = acc + dot(GG[j, r].reshape(T, W2), WO[j * W2 : (j + 1) * W2, :])
+        acc = PJ[r] + dot(GG[opp, r].reshape(T, W2), WO[opp])
         PJ[r] = acc
         sq = acc * acc
         sq_hi = sq.astype(bf16)
@@ -430,9 +471,7 @@
             square_to(dx, r).start()
         return 0
 
-    with jax.named_scope("hfwd0"):
-        forward(0)
-    lax.fori_loop(0, NB, project, 0)
+    lax.fori_loop(0, NB, far, 0)
 
     def finish(r, _):
         with jax.named_scope("sqwait"):
@@ -456,15 +495,22 @@
     for k in range(2):
         to_right(left, k, 4 + k).wait_send()
         to_left(right, 3 - k, 4 + k).wait_send()
-    for dm in range(1, NM):
-        piece_to(dm).wait_send()
-        back_to(dm).wait_send()
+    for dy in range(1, NP):
+        piece_to(dy).wait_send()
+
+    @pl.when(C == 0)
+    def _():
+        piece_to(0).wait_send()
 
     def row_left(z, _):
         row_to(z).wait_send()
         return 0
 
-    lax.fori_loop(Z + 1, NZ, row_left, 0)
+    @pl.when(C == 1)
+    def _():
+        for dm in range(1, NM):
+            back_to(dm).wait_send()
+        lax.fori_loop(Z + 1, NZ, row_left, 0)
 
     def rest(r, _):
         h_right(X, r, 0, 0).wait_send()
@@ -496,7 +542,7 @@
             V((T, D), bf16),
             V((NX, 4, Q, D), bf16),
             V((4, D, W2), bf16),
-            V((1024, 512), bf16),
+            V((NX, W2, 512), bf16),
             V((NB, T, W2), bf16),
             V((NB, T, W2), bf16),
             V((NB, T, W2), bf16),
@@ -509,38 +555,43 @@
             V((NB, 2, T, T), f32),
             V((NX, T, W2), f32),
             V((NB, T, W2), f32),
-            V((NM, MSG, 128), bf16),
+            V((NP, MSG, 128), bf16),
             V((NM, MSG, 128), bf16),
             V((NM, PIECE, 128), f32),
             V((MSG, 128), bf16),
             V((NZ, MSG, 128), bf16),
             V((NM, PIECE, 128), bf16),
-            V((NM, PIECE, 128), bf16),
+            V((NP, PIECE, 128), bf16),
             V((NX, NB, 2, H, W2), bf16),
             V((NB, T, 512), f32),
             V((NB, 8, 128), f32),
             V((3, NB, 8, 128), f32),
             dma((4,)), dma((5,)), dma((5,)),
             dma((6,)), dma((6,)), dma((6,)), dma((6,)),
-            dma((NM,)), dma((NM,)),
+            dma((NP,)), dma((NM,)),
             dma((NZ,)), dma((NZ,)),
-            dma((NM,)), dma((NM,)),
+            dma((NM,)), dma((NP,)),
             dma((NB, 3)), dma((NB, 3)), dma((NB, 3)), dma((NB, 3)),
             dma((3, NB)), dma((3, NB)),
             pltpu.SemaphoreType.REGULAR, pltpu.SemaphoreType.REGULAR,
         ],
         compiler_params=pltpu.CompilerParams(
-            collective_id=0, has_side_effects=True, vmem_limit_bytes=60 * 1024 * 1024
+            collective_id=0, has_side_effects=True, vmem_limit_bytes=40 * 1024 * 1024
         ),
     )(
-        tokens,
-        ing.reshape(1, D),
-        wq, wf, wi, wg,
-        slack.reshape(1, W2),
-        sud[0].T,
-        hgain.reshape(1, 128),
-        wo,
-        ogain.reshape(1, 512),
+        *(
+            pltpu.with_memory_space_constraint(x, pltpu.HBM)
+            for x in (
+                tokens,
+                ing.reshape(1, D),
+                wq, wf, wi, wg,
+                slack.reshape(1, W2),
+                sud[0].T,
+                hgain.reshape(1, 128),
+                wo.reshape(NX, W2, 512),
+                ogain.reshape(1, 512),
+            )
+        )
     )
 
 

time: 61.8 us -> 55.9 us (0.905)
  Pallas kernels: 59.8 us -> 55 us
  local copies, waits for them, and re-layouts: 1.87 us -> 0.8 us
    pallas_call x1, Pallas kernels: 59.8 us -> 55 us  [shards(): pl.pallas_call(body, name='layer', out_shape=jax.ShapeDtypeStruct((1, 512...]
    unnamed x1, local copies, waits for them, and re-layouts: 1.87 us -> 0.8 us
where the time goes in v3:
time: 55.9 us; the launch traced here: 55.8 us
  Pallas kernels  55 us (98%)
  local copies, waits for them, and re-layouts  0.8 us (1%)
    pallas_call x1, Pallas kernels, shards(): pl.pallas_call(body, name='layer', out_shape=jax.ShapeDtypeStruct((1, 512...  55 us

profile of v3, /device:TPU:704, one launch (start us, length us, event | category | flops | bytes accessed | tf_op | source)
XLA Modules:
  0.0 55.8 jit_solution(2934713973609534301)
XLA Ops:
  0.0 55.0 %layer.1 = bf16[1,512,512]{2,1,0:T(8,128)(2,1)S(1)} custom-call(bf16[1,128,2048]{2,1,0:T(8,128)(2,1)} %tokens.1, f32[1,2048]{1,0:T(1,128)} %bitcast.9, bf16[2048,256]{1,0:T(8,128)(2,1)} %wq.1, bf16[2048,256]{1,0:T(8,128)(2,1)} %wf.1, bf16[2048,256]{1,0:T(8,128)(2,1)} %wi.1, bf16[2048,256]{1,0:T(8,128)(2,1)} %wg.1, f32[1,256]{1,0:T(1,128)} %bitcast.12, ...), custom_call_target="tpu_custom_call" | custom-call | tf_op jit(solution)/shard_map/layer/pallas_call | solution.py:534
  55.0 0.8 %copy.13 = bf16[1,512,512]{2,1,0:T(8,128)(2,1)} copy(bf16[1,512,512]{2,1,0:T(8,128)(2,1)S(1)} %layer.1) | data formatting | bytes 1048576

commit v4 on v3

--- a/solution.py
+++ b/solution.py
@@ -66,12 +66,13 @@
     def member(m):
         return {"sp_1": m // NC, "sp_2": lax.rem(m, NC)}
 
-    late = jnp.where(Z == 0, NM - 1, 0)
-    mine = lax.rem(M + late, NM)
-
+    host_y = jnp.where(Z == 0, 0, NY // 2)
+    host_c = jnp.where(Z == 0, 0, 1)
+    hosts_row = (Y == host_y) & (C == host_c)
+    hosts_line = (Z == NZ - 1) & (C == 1)
+    host = host_y * NC + host_c
+    to_hear = 2 + jnp.where(hosts_row, NM - 1, 0) + jnp.where(hosts_line, NZ - 1, 0)
     barrier = pltpu.get_barrier_semaphore()
-    for dx in range(1, NX):
-        pl.semaphore_signal(barrier, inc=1, device_id={"tp": lax.rem(X + dx, NX)}, device_id_type=MESH)
 
     def load_rows(k):
         rows = pl.ds(k * Q, Q)
@@ -85,29 +86,20 @@
     ]
     loads = [pltpu.make_async_copy(w, W.at[i], ldsem.at[i]) for i, w in enumerate((wq, wf, wi, wg))]
     ld_wo = pltpu.make_async_copy(wo, WO, ldsem.at[4])
+    load_rows(0).start()
     small[0].start()
-    for k in OUTER:
+    for side in (right, left):
+        pl.semaphore_signal(barrier, inc=1, device_id={"tp": side}, device_id_type=MESH)
+    for k in OUTER[1:]:
         load_rows(k).start()
-    for c in small[1:]:
-        c.start()
-    for c in loads:
-        c.start()
-    ld_wo.start()
-
-    def greet_row(k, _):
-        pl.semaphore_signal(barrier, inc=1, device_id=member(lax.rem(k + NM - late, NM)), device_id_type=MESH)
-        return 0
-
-    def greet_line(z, _):
-        pl.semaphore_signal(barrier, inc=1, device_id={"sp_0": z}, device_id_type=MESH)
-        return 0
-
-    lax.fori_loop(mine + 1, NM, greet_row, 0)
-
-    @pl.when(C == 1)
-    def _():
-        lax.fori_loop(Z + 1, NZ, greet_line, 0)
-
+
+    @pl.when(jnp.logical_not(hosts_row))
+    def _():
+        pl.semaphore_signal(barrier, inc=1, device_id={"sp_1": host_y, "sp_2": host_c}, device_id_type=MESH)
+
+    @pl.when((Z < NZ - 1) & (C == 1))
+    def _():
+        pl.semaphore_signal(barrier, inc=1, device_id={"sp_0": NZ - 1}, device_id_type=MESH)
 
     small[0].wait()
 
@@ -123,22 +115,29 @@
 
     def to_right(who, k, slot):
         return pltpu.make_async_remote_copy(
-            G.at[who, k], G.at[who, k], gsR.at[slot], grR.at[slot], device_id={"tp": right}, device_id_type=MESH
+            G.at[who, k], G.at[who, k], gsR.at[slot // 4], grR.at[slot], device_id={"tp": right}, device_id_type=MESH
         )
 
     def to_left(who, k, slot):
         return pltpu.make_async_remote_copy(
-            G.at[who, k], G.at[who, k], gsL.at[slot], grL.at[slot], device_id={"tp": left}, device_id_type=MESH
-        )
-
-    load_rows(0).wait()
-    norm_rows(0)
+            G.at[who, k], G.at[who, k], gsL.at[slot // 4], grL.at[slot], device_id={"tp": left}, device_id_type=MESH
+        )
+
+    with jax.named_scope("ld0"):
+        load_rows(0).wait()
+    with jax.named_scope("n0"):
+        norm_rows(0)
+        load_rows(3).wait()
+        norm_rows(3)
     with jax.named_scope("barrier"):
-        pl.semaphore_wait(barrier, (NX - 1) + mine + Z * C)
+        pl.semaphore_wait(barrier, to_hear)
     to_right(X, 0, 0).start()
-    load_rows(3).wait()
-    norm_rows(3)
     to_left(X, 3, 3).start()
+    for c in loads:
+        c.start()
+    for c in small[1:]:
+        c.start()
+    ld_wo.start()
     load_rows(1).wait()
     norm_rows(1)
     to_right(X, 1, 1).start()
@@ -151,19 +150,20 @@
     to_left(X, 0, 0).start()
 
     def ready_row(k, _):
-        pl.semaphore_signal(rdyM, inc=1, device_id=member(lax.rem(k + NM - late, NM)), device_id_type=MESH)
+        pl.semaphore_signal(rdyM, inc=1, device_id=member(lax.rem(host + k, NM)), device_id_type=MESH)
         return 0
 
     def ready_line(z, _):
         pl.semaphore_signal(rdyZ, inc=1, device_id={"sp_0": z}, device_id_type=MESH)
         return 0
 
-    lax.fori_loop(0, mine, ready_row, 0)
-
-    @pl.when(C == 1)
-    def _():
-        lax.fori_loop(0, Z, ready_line, 0)
-
+    @pl.when(hosts_row)
+    def _():
+        lax.fori_loop(1, NM, ready_row, 0)
+
+    @pl.when(hosts_line)
+    def _():
+        lax.fori_loop(0, NZ - 1, ready_line, 0)
 
     for c in small[1:]:
         c.wait()
@@ -277,19 +277,13 @@
 
     def piece_to(dy):
         p = lax.rem(Y + dy, NP)
-        at = 2 * dy + 1 - C
-        return pltpu.make_async_remote_copy(
-            msgA.at[p], rA.at[M], sA.at[dy], qA.at[at], device_id={"sp_1": p, "sp_2": 1}, device_id_type=MESH
-        )
-
-    def piece_from(at):
-        return pltpu.make_async_remote_copy(
-            msgA.at[0], rA.at[M], sA.at[0], qA.at[at], device_id={"sp_1": Y, "sp_2": 1}, device_id_type=MESH
-        )
-
-    @pl.when(mine < NM - 1)
-    def _():
-        pl.semaphore_wait(rdyM, NM - 1 - mine)
+        return pltpu.make_async_remote_copy(
+            msgA.at[p], rA.at[M], sA, qA, device_id={"sp_1": p, "sp_2": 1}, device_id_type=MESH
+        )
+
+    @pl.when(jnp.logical_not(hosts_row))
+    def _():
+        pl.semaphore_wait(rdyM, 1)
 
     for dy in far_first[:-1]:
         piece_to(dy).start()
@@ -301,6 +295,10 @@
     @pl.when(C == 1)
     def _():
         rA[M] = msgA[Y]
+
+    for sem, near_one in ((gsR, left), (gsL, right)):
+        pltpu.make_async_copy(G.at[X], G.at[X], sem.at[0]).wait()
+        pltpu.make_async_copy(G.at[near_one, 0:2], G.at[near_one, 0:2], sem.at[1]).wait()
 
     with jax.named_scope("rest3"):
         block_rest(opp)
@@ -346,13 +344,7 @@
     def back_to(dm):
         m = lax.rem(M + dm, NM)
         return pltpu.make_async_remote_copy(
-            rout.at[m], SIN.at[Y], sR.at[dm], qR.at[Y], device_id=member(m), device_id_type=MESH
-        )
-
-    def back_from(dy):
-        p = lax.rem(Y + dy, NP)
-        return pltpu.make_async_remote_copy(
-            rout.at[0], SIN.at[p], sR.at[0], qR.at[p], device_id={"sp_1": p, "sp_2": 1}, device_id_type=MESH
+            rout.at[m], SIN.at[Y], sR, qR, device_id=member(m), device_id_type=MESH
         )
 
     back_order = sorted(range(1, NM), key=lambda d: -min(d // 2, NY - d // 2))
@@ -360,8 +352,7 @@
     @pl.when(C == 1)
     def _():
         with jax.named_scope("rswait"):
-            for at in range(1, NM):
-                piece_from(at).wait_recv()
+            pltpu.make_async_copy(rA.at[1:NM], rA.at[1:NM], qA).wait()
 
         state = jnp.zeros((PIECE, 128), f32)
         reach = jnp.zeros((1, 128), f32)
@@ -378,7 +369,7 @@
 
         @pl.when(Z < NZ - 1)
         def _():
-            pl.semaphore_wait(rdyZ, NZ - 1 - Z)
+            pl.semaphore_wait(rdyZ, 1)
 
         lax.fori_loop(Z + 1, NZ, send_row, 0)
         with jax.named_scope("zwait"):
@@ -390,22 +381,24 @@
         SIN[Y] = rout[M]
 
     with jax.named_scope("backwait"):
-        for dy in far_first[:-1]:
-            back_from(dy).wait_recv()
+
+        @pl.when(C == 1)
+        def _():
+            pltpu.make_async_copy(SIN.at[1:NP], SIN.at[1:NP], qR).wait()
 
         @pl.when(C == 0)
         def _():
-            back_from(0).wait_recv()
+            pltpu.make_async_copy(SIN, SIN, qR).wait()
 
     def h_right(who, r, half, slot):
         return pltpu.make_async_remote_copy(
-            GG.at[who, r, half], GG.at[who, r, half], hsR.at[r, slot], hrR.at[r, slot],
+            GG.at[who, r, half], GG.at[who, r, half], hsR.at[slot // 2], hrR.at[r, slot],
             device_id={"tp": right}, device_id_type=MESH,
         )
 
     def h_left(who, r, half, slot):
         return pltpu.make_async_remote_copy(
-            GG.at[who, r, half], GG.at[who, r, half], hsL.at[r, slot], hrL.at[r, slot],
+            GG.at[who, r, half], GG.at[who, r, half], hsL.at[slot // 2], hrL.at[r, slot],
             device_id={"tp": left}, device_id_type=MESH,
         )
 
@@ -437,13 +430,27 @@
 
     def square_to(dx, r):
         return pltpu.make_async_remote_copy(
-            sqo.at[r], sqr.at[dx - 1, r], sS.at[dx - 1, r], qS.at[dx - 1, r],
+            sqo.at[r], sqr.at[dx - 1, r], sS, qS.at[dx - 1, r],
             device_id={"tp": lax.rem(X + dx, NX)}, device_id_type=MESH,
         )
 
     for r in range(NB):
         with jax.named_scope("hfwd"):
             forward(r)
+
+    def row_left(z, _):
+        row_to(z).wait_send()
+        return 0
+
+    @pl.when(C == 1)
+    def _():
+        pltpu.make_async_copy(msgA.at[1:NP], msgA.at[1:NP], sA).wait()
+        pltpu.make_async_copy(rout.at[1:NM], rout.at[1:NM], sR).wait()
+        lax.fori_loop(Z + 1, NZ, row_left, 0)
+
+    @pl.when(C == 0)
+    def _():
+        pltpu.make_async_copy(msgA, msgA, sA).wait()
 
     def near(r, _):
         with jax.named_scope("hnear"):
@@ -473,6 +480,10 @@
 
     lax.fori_loop(0, NB, far, 0)
 
+    for sem in (hsR, hsL):
+        pltpu.make_async_copy(GG.at[X], GG.at[X], sem.at[0]).wait()
+        pltpu.make_async_copy(GG.at[X, 0:2], GG.at[X, 0:2], sem.at[1]).wait()
+
     def finish(r, _):
         with jax.named_scope("sqwait"):
             for dx in (1, 2, 3):
@@ -489,41 +500,8 @@
 
     lax.fori_loop(0, NB, finish, 0)
 
-    for k in range(4):
-        to_right(X, k, k).wait_send()
-        to_left(X, k, k).wait_send()
-    for k in range(2):
-        to_right(left, k, 4 + k).wait_send()
-        to_left(right, 3 - k, 4 + k).wait_send()
-    for dy in range(1, NP):
-        piece_to(dy).wait_send()
-
-    @pl.when(C == 0)
-    def _():
-        piece_to(0).wait_send()
-
-    def row_left(z, _):
-        row_to(z).wait_send()
-        return 0
-
-    @pl.when(C == 1)
-    def _():
-        for dm in range(1, NM):
-            back_to(dm).wait_send()
-        lax.fori_loop(Z + 1, NZ, row_left, 0)
-
-    def rest(r, _):
-        h_right(X, r, 0, 0).wait_send()
-        h_right(X, r, 1, 1).wait_send()
-        h_right(left, r, 0, 2).wait_send()
-        h_left(X, r, 1, 0).wait_send()
-        h_left(X, r, 0, 1).wait_send()
-        h_left(right, r, 1, 2).wait_send()
-        for dx in (1, 2, 3):
-            square_to(dx, r).wait_send()
-        return 0
-
-    lax.fori_loop(0, NB, rest, 0)
+    with jax.named_scope("end"):
+        pltpu.make_async_copy(sqr, sqr, sS).wait()
 
 
 def shards(tokens, ing, wq, wf, wi, wg, slack, sud, hgain, wo, ogain):
@@ -567,12 +545,12 @@
             V((NB, 8, 128), f32),
             V((3, NB, 8, 128), f32),
             dma((4,)), dma((5,)), dma((5,)),
-            dma((6,)), dma((6,)), dma((6,)), dma((6,)),
-            dma((NP,)), dma((NM,)),
+            dma((2,)), dma((6,)), dma((2,)), dma((6,)),
+            dma, dma,
             dma((NZ,)), dma((NZ,)),
-            dma((NM,)), dma((NP,)),
-            dma((NB, 3)), dma((NB, 3)), dma((NB, 3)), dma((NB, 3)),
-            dma((3, NB)), dma((3, NB)),
+            dma, dma,
+            dma((2,)), dma((NB, 3)), dma((2,)), dma((NB, 3)),
+            dma, dma((3, NB)),
             pltpu.SemaphoreType.REGULAR, pltpu.SemaphoreType.REGULAR,
         ],
         compiler_params=pltpu.CompilerParams(

time: 55.9 us -> 54.3 us (0.971)
  Pallas kernels: 55 us -> 53.3 us
    pallas_call x1, Pallas kernels: 55 us -> 53.3 us  [shards(): pl.pallas_call(body, name='layer', out_shape=jax.ShapeDtypeStruct((1, 512...]
where the time goes in v4:
time: 54.3 us; the launch traced here: 54.1 us
  Pallas kernels  53.3 us (98%)
  local copies, waits for them, and re-layouts  0.8 us (1%)
    pallas_call x1, Pallas kernels, shards(): pl.pallas_call(body, name='layer', out_shape=jax.ShapeDtypeStruct((1, 512...  53.3 us

profile of v4, /device:TPU:704, one launch (start us, length us, event | category | flops | bytes accessed | tf_op | source)
XLA Modules:
  0.0 54.1 jit_solution(16174263368046388698)
XLA Ops:
  0.0 53.3 %layer.1 = bf16[1,512,512]{2,1,0:T(8,128)(2,1)S(1)} custom-call(bf16[1,128,2048]{2,1,0:T(8,128)(2,1)} %tokens.1, f32[1,2048]{1,0:T(1,128)} %bitcast.9, bf16[2048,256]{1,0:T(8,128)(2,1)} %wq.1, bf16[2048,256]{1,0:T(8,128)(2,1)} %wf.1, bf16[2048,256]{1,0:T(8,128)(2,1)} %wi.1, bf16[2048,256]{1,0:T(8,128)(2,1)} %wg.1, f32[1,256]{1,0:T(1,128)} %bitcast.12, ...), custom_call_target="tpu_custom_call" | custom-call | tf_op jit(solution)/shard_map/layer/pallas_call | solution.py:512
  53.3 0.8 %copy.13 = bf16[1,512,512]{2,1,0:T(8,128)(2,1)} copy(bf16[1,512,512]{2,1,0:T(8,128)(2,1)S(1)} %layer.1) | data formatting | bytes 1048576

commit v5 on v4

--- a/solution.py
+++ b/solution.py
@@ -50,7 +50,7 @@
 def body(
     tokens, ing_in, wq, wf, wi, wg, slack_in, sud_in, hgain_in, wo, ogain_in, out,
     ing, slack, sud, hgain, ogain,
-    xin, G, W, WO, lqA, lk, vv, lqD, gs, ST, PB, DT, DP, BC, AA, O,
+    xin, G, W, WO, lqA, lk, vv, lqD, gs, ST, PB, DT, DP, BC, AA, WK, O,
     msgA, rA, Pp, zout, rz, rout, SIN, GG, PJ, sqo, sqr,
     tksem, smsem, ldsem, gsR, grR, gsL, grL, sA, qA, sZ, qZ, sR, qR, hsR, hrR, hsL, hrL, sS, qS, rdyM, rdyZ,
 ):
@@ -193,7 +193,7 @@
         a_lo = (a - a_hi.astype(f32)).astype(bf16)
         A = dot(tri, a_hi) + dot(tri, a_lo)
         AA[b] = A
-        lk[b] = (w * jnp.exp(-A)).astype(bf16)
+        WK[b] = w
         for h in range(2):
             cols = slice(h * 128, (h + 1) * 128)
             reach = A[:, cols] + BC[b, h]
@@ -205,6 +205,7 @@
     def block_rest(b):
         x = G[b].reshape(T, D)
         q_raw = dot(x, W[0]).astype(bf16).astype(f32) * KEY ** (-0.5)
+        lk[b] = (WK[b] * jnp.exp(-AA[b])).astype(bf16)
         q_in = q_raw * jnp.exp(AA[b])
         lqA[b] = q_in.astype(bf16)
         for h in range(2):
@@ -390,15 +391,15 @@
         def _():
             pltpu.make_async_copy(SIN, SIN, qR).wait()
 
-    def h_right(who, r, half, slot):
-        return pltpu.make_async_remote_copy(
-            GG.at[who, r, half], GG.at[who, r, half], hsR.at[slot // 2], hrR.at[r, slot],
+    def h_right(who, r, half, slot, on):
+        return pltpu.make_async_remote_copy(
+            GG.at[who, r, half], GG.at[who, r, half], hsR.at[on], hrR.at[r, slot],
             device_id={"tp": right}, device_id_type=MESH,
         )
 
-    def h_left(who, r, half, slot):
-        return pltpu.make_async_remote_copy(
-            GG.at[who, r, half], GG.at[who, r, half], hsL.at[slot // 2], hrL.at[r, slot],
+    def h_left(who, r, half, slot, on):
+        return pltpu.make_async_remote_copy(
+            GG.at[who, r, half], GG.at[who, r, half], hsL.at[on], hrL.at[r, slot],
             device_id={"tp": left}, device_id_type=MESH,
         )
 
@@ -412,10 +413,10 @@
             parts.append(o * gs[r, :, cols])
         gated = jnp.concatenate(parts, axis=1).astype(bf16)
         GG[X, r] = gated.reshape(2, H, W2)
-        h_right(X, r, 0, 0).start()
-        h_left(X, r, 1, 0).start()
-        h_right(X, r, 1, 1).start()
-        h_left(X, r, 0, 1).start()
+        h_right(X, r, 0, 0, 0).start()
+        h_left(X, r, 1, 0, 0).start()
+        h_right(X, r, 1, 1, 0).start()
+        h_left(X, r, 0, 1, 0).start()
         return 0
 
     with jax.named_scope("readout"):
@@ -423,14 +424,14 @@
         ld_wo.wait()
 
     def forward(r):
-        h_right(X, r, 0, 0).wait_recv()
-        h_right(left, r, 0, 2).start()
-        h_left(X, r, 1, 0).wait_recv()
-        h_left(right, r, 1, 2).start()
+        h_right(X, r, 0, 0, 0).wait_recv()
+        h_right(left, r, 0, 2, 1).start()
+        h_left(X, r, 1, 0, 0).wait_recv()
+        h_left(right, r, 1, 2, 1).start()
 
     def square_to(dx, r):
         return pltpu.make_async_remote_copy(
-            sqo.at[r], sqr.at[dx - 1, r], sS, qS.at[dx - 1, r],
+            sqo.at[r], sqr.at[r, dx - 1], sS, qS.at[r],
             device_id={"tp": lax.rem(X + dx, NX)}, device_id_type=MESH,
         )
 
@@ -454,8 +455,8 @@
 
     def near(r, _):
         with jax.named_scope("hnear"):
-            h_right(X, r, 1, 1).wait_recv()
-            h_left(X, r, 0, 1).wait_recv()
+            h_right(X, r, 1, 1, 0).wait_recv()
+            h_left(X, r, 0, 1, 0).wait_recv()
         acc = dot(GG[X, r].reshape(T, W2), WO[X])
         acc = acc + dot(GG[left, r].reshape(T, W2), WO[left])
         PJ[r] = acc + dot(GG[right, r].reshape(T, W2), WO[right])
@@ -465,14 +466,15 @@
 
     def far(r, _):
         with jax.named_scope("hfar"):
-            h_right(left, r, 0, 2).wait_recv()
-            h_left(right, r, 1, 2).wait_recv()
+            h_right(left, r, 0, 2, 1).wait_recv()
+            h_left(right, r, 1, 2, 1).wait_recv()
         acc = PJ[r] + dot(GG[opp, r].reshape(T, W2), WO[opp])
         PJ[r] = acc
         sq = acc * acc
+        sq = (sq[:, 0:128] + sq[:, 128:256]) + (sq[:, 256:384] + sq[:, 384:512])
         sq_hi = sq.astype(bf16)
         sq_lo = (sq - sq_hi.astype(f32)).astype(bf16)
-        ones = jnp.ones((8, 512), f32).astype(bf16)
+        ones = jnp.ones((8, 128), f32).astype(bf16)
         sqo[r] = dot(ones, sq_hi, 1, 1) + dot(ones, sq_lo, 1, 1)
         for dx in (2, 1, 3):
             square_to(dx, r).start()
@@ -486,9 +488,8 @@
 
     def finish(r, _):
         with jax.named_scope("sqwait"):
-            for dx in (1, 2, 3):
-                square_to(dx, r).wait_recv()
-        total = sqo[r] + sqr[0, r] + sqr[1, r] + sqr[2, r]
+            pltpu.make_async_copy(sqr.at[r], sqr.at[r], qS.at[r]).wait()
+        total = sqo[r] + sqr[r, 0] + sqr[r, 1] + sqr[r, 2]
         scale = lax.rsqrt(total[0:1, :] / D + EPS)
         scale = jnp.broadcast_to(scale, (T, T)).T
         for j in range(4):
@@ -532,6 +533,7 @@
             V((NB, 2, 128), f32),
             V((NB, 2, T, T), f32),
             V((NX, T, W2), f32),
+            V((NX, T, W2), f32),
             V((NB, T, W2), f32),
             V((NP, MSG, 128), bf16),
             V((NM, MSG, 128), bf16),
@@ -543,14 +545,14 @@
             V((NX, NB, 2, H, W2), bf16),
             V((NB, T, 512), f32),
             V((NB, 8, 128), f32),
-            V((3, NB, 8, 128), f32),
+            V((NB, 3, 8, 128), f32),
             dma((4,)), dma((5,)), dma((5,)),
             dma((2,)), dma((6,)), dma((2,)), dma((6,)),
             dma, dma,
             dma((NZ,)), dma((NZ,)),
             dma, dma,
             dma((2,)), dma((NB, 3)), dma((2,)), dma((NB, 3)),
-            dma, dma((3, NB)),
+            dma, dma((NB,)),
             pltpu.SemaphoreType.REGULAR, pltpu.SemaphoreType.REGULAR,
         ],
         compiler_params=pltpu.CompilerParams(

time: 54.3 us -> 54.1 us (level)
  no operation moved by 1% of the time
where the time goes in v5:
time: 54.1 us; the launch traced here: 53.9 us
  Pallas kernels  53.1 us (98%)
  local copies, waits for them, and re-layouts  0.8 us (1%)
    pallas_call x1, Pallas kernels, shards(): pl.pallas_call(body, name='layer', out_shape=jax.ShapeDtypeStruct((1, 512...  53.1 us

profile of v5, /device:TPU:704, one launch (start us, length us, event | category | flops | bytes accessed | tf_op | source)
XLA Modules:
  0.0 53.9 jit_solution(14538127343315072084)
XLA Ops:
  0.0 53.1 %layer.1 = bf16[1,512,512]{2,1,0:T(8,128)(2,1)S(1)} custom-call(bf16[1,128,2048]{2,1,0:T(8,128)(2,1)} %tokens.1, f32[1,2048]{1,0:T(1,128)} %bitcast.9, bf16[2048,256]{1,0:T(8,128)(2,1)} %wq.1, bf16[2048,256]{1,0:T(8,128)(2,1)} %wf.1, bf16[2048,256]{1,0:T(8,128)(2,1)} %wi.1, bf16[2048,256]{1,0:T(8,128)(2,1)} %wg.1, f32[1,256]{1,0:T(1,128)} %bitcast.12, ...), custom_call_target="tpu_custom_call" | custom-call | tf_op jit(solution)/shard_map/layer/pallas_call | solution.py:513
  53.1 0.8 %copy.13 = bf16[1,512,512]{2,1,0:T(8,128)(2,1)} copy(bf16[1,512,512]{2,1,0:T(8,128)(2,1)S(1)} %layer.1) | data formatting | bytes 1048576

commit v6 on v5

--- a/solution.py
+++ b/solution.py
@@ -51,8 +51,8 @@
     tokens, ing_in, wq, wf, wi, wg, slack_in, sud_in, hgain_in, wo, ogain_in, out,
     ing, slack, sud, hgain, ogain,
     xin, G, W, WO, lqA, lk, vv, lqD, gs, ST, PB, DT, DP, BC, AA, WK, O,
-    msgA, rA, Pp, zout, rz, rout, SIN, GG, PJ, sqo, sqr,
-    tksem, smsem, ldsem, gsR, grR, gsL, grL, sA, qA, sZ, qZ, sR, qR, hsR, hrR, hsL, hrL, sS, qS, rdyM, rdyZ,
+    FS, TR, NI, msgA, rA, Pp, zout, rz, rout, SIN, GG, PJ, sqo, sqr,
+    tksem, smsem, ldsem, gsR, grR, gsL, grL, sA, qA, sZ, qZ, sR, qR, sN, qN, hsR, hrR, hsL, hrL, sS, qS, rdyM, rdyZ,
 ):
     X = lax.axis_index("tp")
     Z = lax.axis_index("sp_0")
@@ -66,14 +66,15 @@
     def member(m):
         return {"sp_1": m // NC, "sp_2": lax.rem(m, NC)}
 
+    barrier = pltpu.get_barrier_semaphore()
+    for side in (right, left):
+        pl.semaphore_signal(barrier, inc=1, device_id={"tp": side}, device_id_type=MESH)
     host_y = jnp.where(Z == 0, 0, NY // 2)
     host_c = jnp.where(Z == 0, 0, 1)
     hosts_row = (Y == host_y) & (C == host_c)
     hosts_line = (Z == NZ - 1) & (C == 1)
     host = host_y * NC + host_c
     to_hear = 2 + jnp.where(hosts_row, NM - 1, 0) + jnp.where(hosts_line, NZ - 1, 0)
-    barrier = pltpu.get_barrier_semaphore()
-
     def load_rows(k):
         rows = pl.ds(k * Q, Q)
         return pltpu.make_async_copy(tokens.at[0, rows], xin.at[rows], tksem.at[k])
@@ -84,12 +85,10 @@
             ((ing_in, ing), (slack_in, slack), (sud_in, sud), (hgain_in, hgain), (ogain_in, ogain))
         )
     ]
-    loads = [pltpu.make_async_copy(w, W.at[i], ldsem.at[i]) for i, w in enumerate((wq, wf, wi, wg))]
-    ld_wo = pltpu.make_async_copy(wo, WO, ldsem.at[4])
+    loads = [pltpu.make_async_copy(w, W.at[i], ldsem.at[0]) for i, w in enumerate((wq, wf, wi, wg))]
+    ld_wo = pltpu.make_async_copy(wo, WO, ldsem.at[1])
     load_rows(0).start()
     small[0].start()
-    for side in (right, left):
-        pl.semaphore_signal(barrier, inc=1, device_id={"tp": side}, device_id_type=MESH)
     for k in OUTER[1:]:
         load_rows(k).start()
 
@@ -179,8 +178,7 @@
             BC[b, h] = jnp.broadcast_to(total, (T, T))
 
     with jax.named_scope("wload"):
-        for c in loads:
-            c.wait()
+        pltpu.make_async_copy(W, W, ldsem.at[0]).wait()
 
     def block_state(b):
         x = G[b].reshape(T, D)
@@ -267,6 +265,8 @@
             reach = reach + step
         finals.append(state)
         totals.append(reach)
+        FS[h] = state
+        TR[h : h + 1, :] = reach
     for h in range(2):
         rows = decay_rows(totals[h])
         for j in range(NP // 2):
@@ -342,13 +342,14 @@
         rows = rz[z]
         return jnp.exp(decay_of(rows)) * before + rows[0:PIECE, :].astype(f32)
 
-    def back_to(dm):
-        m = lax.rem(M + dm, NM)
-        return pltpu.make_async_remote_copy(
-            rout.at[m], SIN.at[Y], sR, qR, device_id=member(m), device_id_type=MESH
-        )
-
-    back_order = sorted(range(1, NM), key=lambda d: -min(d // 2, NY - d // 2))
+    def back_to(dy):
+        y = lax.rem(Y + dy, NY)
+        return pltpu.make_async_remote_copy(
+            rout.at[y], SIN.at[Y], sR, qR, device_id={"sp_1": y, "sp_2": 0}, device_id_type=MESH
+        )
+
+    def pass_on():
+        return pltpu.make_async_remote_copy(NI, SIN, sN, qN, device_id={"sp_2": 1}, device_id_type=MESH)
 
     @pl.when(C == 1)
     def _():
@@ -375,31 +376,37 @@
         lax.fori_loop(Z + 1, NZ, send_row, 0)
         with jax.named_scope("zwait"):
             before = lax.fori_loop(0, Z, take_row, jnp.zeros((PIECE, 128), f32))
-        for m in range(NM):
-            rout[m] = (jnp.exp(reaches[m]) * before + Pp[m]).astype(bf16)
-        for dm in back_order:
-            back_to(dm).start()
-        SIN[Y] = rout[M]
+        for y in range(NY):
+            rout[y] = (jnp.exp(reaches[NC * y]) * before + Pp[NC * y]).astype(bf16)
+        for dy in far_first:
+            back_to(dy).start()
 
     with jax.named_scope("backwait"):
-
-        @pl.when(C == 1)
-        def _():
-            pltpu.make_async_copy(SIN.at[1:NP], SIN.at[1:NP], qR).wait()
 
         @pl.when(C == 0)
         def _():
             pltpu.make_async_copy(SIN, SIN, qR).wait()
+            for h in range(2):
+                keep = jnp.exp(TR[h : h + 1, :])
+                for j in range(NP // 2):
+                    p = h * (NP // 2) + j
+                    mine = FS[h, j * PIECE : (j + 1) * PIECE, :]
+                    NI[p] = (keep * SIN[p].astype(f32) + mine).astype(bf16)
+            pass_on().start()
+
+        @pl.when(C == 1)
+        def _():
+            pass_on().wait_recv()
 
     def h_right(who, r, half, slot, on):
         return pltpu.make_async_remote_copy(
-            GG.at[who, r, half], GG.at[who, r, half], hsR.at[on], hrR.at[r, slot],
+            GG.at[who, r, half], GG.at[who, r, half], hsR.at[on], hrR.at[slot],
             device_id={"tp": right}, device_id_type=MESH,
         )
 
     def h_left(who, r, half, slot, on):
         return pltpu.make_async_remote_copy(
-            GG.at[who, r, half], GG.at[who, r, half], hsL.at[on], hrL.at[r, slot],
+            GG.at[who, r, half], GG.at[who, r, half], hsL.at[on], hrL.at[slot],
             device_id={"tp": left}, device_id_type=MESH,
         )
 
@@ -413,10 +420,10 @@
             parts.append(o * gs[r, :, cols])
         gated = jnp.concatenate(parts, axis=1).astype(bf16)
         GG[X, r] = gated.reshape(2, H, W2)
-        h_right(X, r, 0, 0, 0).start()
-        h_left(X, r, 1, 0, 0).start()
-        h_right(X, r, 1, 1, 0).start()
-        h_left(X, r, 0, 1, 0).start()
+        h_right(X, r, 0, r, 0).start()
+        h_left(X, r, 1, r, 0).start()
+        h_right(X, r, 1, 8, 0).start()
+        h_left(X, r, 0, 8, 0).start()
         return 0
 
     with jax.named_scope("readout"):
@@ -424,10 +431,10 @@
         ld_wo.wait()
 
     def forward(r):
-        h_right(X, r, 0, 0, 0).wait_recv()
-        h_right(left, r, 0, 2, 1).start()
-        h_left(X, r, 1, 0, 0).wait_recv()
-        h_left(right, r, 1, 2, 1).start()
+        h_right(X, r, 0, r, 0).wait_recv()
+        h_right(left, r, 0, NB + r, 1).start()
+        h_left(X, r, 1, r, 0).wait_recv()
+        h_left(right, r, 1, NB + r, 1).start()
 
     def square_to(dx, r):
         return pltpu.make_async_remote_copy(
@@ -446,17 +453,19 @@
     @pl.when(C == 1)
     def _():
         pltpu.make_async_copy(msgA.at[1:NP], msgA.at[1:NP], sA).wait()
-        pltpu.make_async_copy(rout.at[1:NM], rout.at[1:NM], sR).wait()
+        pltpu.make_async_copy(rout, rout, sR).wait()
         lax.fori_loop(Z + 1, NZ, row_left, 0)
 
     @pl.when(C == 0)
     def _():
         pltpu.make_async_copy(msgA, msgA, sA).wait()
+        pass_on().wait_send()
+
+    with jax.named_scope("hnear"):
+        for sem in (hrR, hrL):
+            pltpu.make_async_copy(GG.at[X, 0:2], GG.at[X, 0:2], sem.at[2 * NB]).wait()
 
     def near(r, _):
-        with jax.named_scope("hnear"):
-            h_right(X, r, 1, 1, 0).wait_recv()
-            h_left(X, r, 0, 1, 0).wait_recv()
         acc = dot(GG[X, r].reshape(T, W2), WO[X])
         acc = acc + dot(GG[left, r].reshape(T, W2), WO[left])
         PJ[r] = acc + dot(GG[right, r].reshape(T, W2), WO[right])
@@ -466,8 +475,8 @@
 
     def far(r, _):
         with jax.named_scope("hfar"):
-            h_right(left, r, 0, 2, 1).wait_recv()
-            h_left(right, r, 1, 2, 1).wait_recv()
+            h_right(left, r, 0, NB + r, 1).wait_recv()
+            h_left(right, r, 1, NB + r, 1).wait_recv()
         acc = PJ[r] + dot(GG[opp, r].reshape(T, W2), WO[opp])
         PJ[r] = acc
         sq = acc * acc
@@ -535,23 +544,26 @@
             V((NX, T, W2), f32),
             V((NX, T, W2), f32),
             V((NB, T, W2), f32),
+            V((2, 128, 128), f32),
+            V((2, 128), f32),
+            V((NP, PIECE, 128), bf16),
             V((NP, MSG, 128), bf16),
             V((NM, MSG, 128), bf16),
             V((NM, PIECE, 128), f32),
             V((MSG, 128), bf16),
             V((NZ, MSG, 128), bf16),
-            V((NM, PIECE, 128), bf16),
+            V((NP, PIECE, 128), bf16),
             V((NP, PIECE, 128), bf16),
             V((NX, NB, 2, H, W2), bf16),
             V((NB, T, 512), f32),
             V((NB, 8, 128), f32),
             V((NB, 3, 8, 128), f32),
-            dma((4,)), dma((5,)), dma((5,)),
+            dma((4,)), dma((5,)), dma((2,)),
             dma((2,)), dma((6,)), dma((2,)), dma((6,)),
             dma, dma,
             dma((NZ,)), dma((NZ,)),
-            dma, dma,
-            dma((2,)), dma((NB, 3)), dma((2,)), dma((NB, 3)),
+            dma, dma, dma, dma,
+            dma((2,)), dma((2 * NB + 1,)), dma((2,)), dma((2 * NB + 1,)),
             dma, dma((NB,)),
             pltpu.SemaphoreType.REGULAR, pltpu.SemaphoreType.REGULAR,
         ],

time: 54.1 us -> 53 us (0.980)
  Pallas kernels: 53.1 us -> 52.1 us
    pallas_call x1, Pallas kernels: 53.1 us -> 52.1 us  [shards(): pl.pallas_call(body, name='layer', out_shape=jax.ShapeDtypeStruct((1, 512...]
where the time goes in v6:
time: 53 us; the launch traced here: 52.9 us
  Pallas kernels  52.1 us (98%)
  local copies, waits for them, and re-layouts  0.8 us (2%)
    pallas_call x1, Pallas kernels, shards(): pl.pallas_call(body, name='layer', out_shape=jax.ShapeDtypeStruct((1, 512...  52.1 us

profile of v6, /device:TPU:704, one launch (start us, length us, event | category | flops | bytes accessed | tf_op | source)
XLA Modules:
  0.0 52.9 jit_solution(12760651760337937875)
XLA Ops:
  0.0 52.1 %layer.1 = bf16[1,512,512]{2,1,0:T(8,128)(2,1)S(1)} custom-call(bf16[1,128,2048]{2,1,0:T(8,128)(2,1)} %tokens.1, f32[1,2048]{1,0:T(1,128)} %bitcast.9, bf16[2048,256]{1,0:T(8,128)(2,1)} %wq.1, bf16[2048,256]{1,0:T(8,128)(2,1)} %wf.1, bf16[2048,256]{1,0:T(8,128)(2,1)} %wi.1, bf16[2048,256]{1,0:T(8,128)(2,1)} %wg.1, f32[1,256]{1,0:T(1,128)} %bitcast.12, ...), custom_call_target="tpu_custom_call" | custom-call | tf_op jit(solution)/shard_map/layer/pallas_call | solution.py:522
  52.1 0.8 %copy.13 = bf16[1,512,512]{2,1,0:T(8,128)(2,1)} copy(bf16[1,512,512]{2,1,0:T(8,128)(2,1)S(1)} %layer.1) | data formatting | bytes 1048576
